TPU v7x, 32 devices: a whole 2x2x4 slice. The times are simulated.
32 devices in a mesh: fs: 8 (over z, x), tp: 4 (over y, core).
Axes of the slice: x: 2, y: 2, z: 4, core: 2. Of those that a mesh axis runs over, the one named last changes fastest.
Arguments:
- tokens: bfloat16 [8192, 2048], P(('fs', 'tp')), may hold values from -6 to 6
- gate_pre: bfloat16 [8192, 5632], P('fs', 'tp'), may hold values from -6 to 6
- value_pre: bfloat16 [8192, 5632], P('fs', 'tp'), may hold values from -6 to 6
- up_gate_w: bfloat16 [2048, 5632], P('fs', 'tp'), may hold values from -0.078125 to 0.078125
- up_value_w: bfloat16 [2048, 5632], P('fs', 'tp'), may hold values from -0.078125 to 0.078125
- conv_weight: float32 [3, 5632], P(None, 'tp'), may hold values from -3 to 3
- conv_bias: float32 [5632], P('tp'), may hold values from -3 to 3
- hidden_grad: bfloat16 [8192, 5632], P('fs', 'tp'), may hold values from -6 to 6
Outputs:
- input_grad: bfloat16 [8192, 2048], P(('fs', 'tp'))
- up_gate_grad: float32 [2048, 5632], P('fs', 'tp')
- up_value_grad: float32 [2048, 5632], P('fs', 'tp')
- conv_weight_grad: float32 [3, 5632], P(None, 'tp')
- conv_bias_grad: float32 [5632], P('tp')
All inputs are finite; a program needn't handle non-finite values.
Results may differ from a plain program's by a relative error of at most 0.013.
Values may be sent and summed in bfloat16 or wider, within the bound.
A program may use at most 128 MiB of HBM per device.

v0:
```python
import jax
import jax.numpy as jnp
from jax import lax
from jax.sharding import PartitionSpec as P


def contract_rows(left, right):
    return lax.dot_general(
        left, right, (((0,), (0,)), ((), ())), preferred_element_type=jnp.float32
    )


def contract_cols(left, right):
    return lax.dot_general(
        left, right, (((1,), (1,)), ((), ())), preferred_element_type=jnp.float32
    )


def ring_of(count):
    return [*range(0, count, 2), *reversed(range(1, count, 2))]


def ring_hops(blocks, axis, backward, steps):
    ring = ring_of(lax.axis_size(axis))
    if backward:
        ring = ring[::-1]
    hops = list(zip(ring, ring[1:] + ring[:1]))
    for _ in range(steps):
        blocks = [*blocks, lax.ppermute(blocks[-1], axis, hops)]
    return blocks


def ring_join(blocks, axis, backward):
    count = lax.axis_size(axis)
    ring = ring_of(count)
    if backward:
        ring = ring[::-1]
    place = [ring.index(i) for i in range(count)]
    mine = jnp.asarray(place, jnp.int32)[lax.axis_index(axis)]
    order = jnp.asarray(ring, jnp.int32)
    rows = blocks[0].shape[0]
    whole = jnp.zeros((rows * count, blocks[0].shape[1]), blocks[0].dtype)
    for step, block in enumerate(blocks):
        owner = order[(mine - step + count) % count]
        whole = lax.dynamic_update_slice(whole, block, (owner * rows, 0))
    return whole


def sum_over(terms, axis):
    count = lax.axis_size(axis)
    if count & (count - 1):
        return lax.psum(terms, axis)
    reach = 1
    while reach < count:
        terms = terms + lax.ppermute(terms, axis, [(i, i ^ reach) for i in range(count)])
        reach *= 2
    return terms


def on_device(
    tokens, gate_pre, value_pre, up_gate_w, up_value_w, conv_weight, conv_bias, hidden_grad
):
    length = gate_pre.shape[0]
    col_count = gate_pre.shape[1]
    scale = float(length * lax.axis_size("fs")) ** (-0.5)
    gate_float = gate_pre.astype(jnp.float32)
    padded = jnp.pad(gate_float, ((2, 0), (0, 0)))
    gate_conv = (
        conv_bias
        + conv_weight[0] * padded[:length]
        + conv_weight[1] * padded[1 : length + 1]
        + conv_weight[2] * padded[2:]
    )
    active, gelu_back = jax.vjp(jax.nn.gelu, gate_conv)
    grad_float = hidden_grad.astype(jnp.float32)
    value_grad = (grad_float * active).astype(jnp.bfloat16)
    conv_grad = gelu_back(grad_float * value_pre.astype(jnp.float32))[0]
    shifted = jnp.pad(conv_grad, ((0, 2), (0, 0)))
    gate_grad = (
        conv_weight[2] * conv_grad
        + conv_weight[1] * shifted[1 : length + 1]
        + conv_weight[0] * shifted[2:]
    ).astype(jnp.bfloat16)
    conv_terms = jnp.stack(
        [
            jnp.sum(conv_grad * padded[:length], axis=0),
            jnp.sum(conv_grad * padded[1 : length + 1], axis=0),
            jnp.sum(conv_grad * padded[2:], axis=0),
            jnp.sum(conv_grad, axis=0),
        ]
    )
    conv_total = sum_over(conv_terms, "fs") * scale
    whole_tokens = lax.all_gather(tokens, "tp", axis=0, tiled=True)
    count = lax.axis_size("fs")
    early = min(2, count - 1)
    gate_blocks = ring_hops([up_gate_w], "fs", False, early)
    value_blocks = ring_hops([up_value_w], "fs", True, early)
    whole_tokens, gate_blocks[-1], value_blocks[-1] = lax.optimization_barrier(
        (whole_tokens, gate_blocks[-1], value_blocks[-1])
    )
    terms = [
        contract_rows(whole_tokens, grad).astype(jnp.bfloat16) for grad in (gate_grad, value_grad)
    ]
    gate_blocks[-1], value_blocks[-1], _ = lax.optimization_barrier(
        (gate_blocks[-1], value_blocks[-1], terms[0][:1, :1])
    )
    gate_blocks = ring_hops(gate_blocks, "fs", False, count - 1 - early)
    value_blocks = ring_hops(value_blocks, "fs", True, count - 1 - early)
    full_gate = ring_join(gate_blocks, "fs", False)
    full_value = ring_join(value_blocks, "fs", True)
    gate_out, value_out = (
        lax.psum_scatter(
            term,
            "fs",
            scatter_dimension=0,
            tiled=True,
        ).astype(jnp.float32)
        * scale
        for term in terms
    )
    input_grad = lax.psum_scatter(
        (contract_cols(gate_grad, full_gate) + contract_cols(value_grad, full_value)).astype(
            jnp.bfloat16
        ),
        "tp",
        scatter_dimension=0,
        tiled=True,
    )
    return (input_grad, gate_out, value_out, conv_total[:3], conv_total[3])


def solution(mesh):
    return jax.shard_map(
        on_device,
        mesh=mesh,
        in_specs=(
            P(("fs", "tp"), None),
            P("fs", "tp"),
            P("fs", "tp"),
            P("fs", "tp"),
            P("fs", "tp"),
            P(None, "tp"),
            P("tp"),
            P("fs", "tp"),
        ),
        out_specs=(P(("fs", "tp"), None), P("fs", "tp"), P("fs", "tp"), P(None, "tp"), P("tp")),
        check_vma=False,
    )
```

profile of v0, /device:TPU:0, one launch (start us, length us, event | category | flops | bytes accessed | tf_op | source)
XLA Modules:
  0.0 393.0 jit_solution(17985406050080118805)
XLA Ops:
  7.2 0.7 all-gather.2.cloned.1.call-update
  8.0 3.0 collective-permute-start.2
  11.0 0.2 collective-permute-start
  11.2 2.2 convert_element_type.36
  13.5 9.3 %multiply_reduce_fusion.2 = (f32[1408]{0:T(1024)S(1)}, f32[1408]{0:T(1024)S(1)}, f32[1408]{0:T(1024)S(1)}, f32[1408]{0:T(1024)S(1)}, f32[1024,1408]{1,0:T(8,128)S(1)}, /*index=5*/f32[1024,1408]{1,0:T(8,128)}) fusion(f32[1024,1408]{1,0:T(8,128)S(1)} %convert_element_type.36, bf16[1024,1408]{1,0:T(8,128)(2,1)S(1)} %copy-done, ...), kind=kLoop, calls=%fused_computation.16 | loop fusion | flops 51898880 | bytes 25997312 | tf_op jit(solution)/shard_map/reduce_sum | solution.py:86
  22.8 6.0 %collective-permute-done = bf16[256,1408]{1,0:T(8,128)(2,1)S(1)} collective-permute-done((bf16[256,1408]{1,0:T(8,128)(2,1)}, bf16[256,1408]{1,0:T(8,128)(2,1)S(1)}, u32[]{:S(2)}, u32[]{:S(2)}) %collective-permute-start) | collective-permute-done | bytes 720928 | tf_op jit(solution)/shard_map/ppermute | solution.py:29
  28.8 0.4 collective-permute-start.1
  29.3 1.6 collective-permute-start.3
  30.9 1.8 add_convert_fusion.1
  32.7 12.9 %collective-permute-done.1 = bf16[256,1408]{1,0:T(8,128)(2,1)S(1)} collective-permute-done((bf16[256,1408]{1,0:T(8,128)(2,1)S(1)}, bf16[256,1408]{1,0:T(8,128)(2,1)S(1)}, u32[]{:S(2)}, u32[]{:S(2)}) %collective-permute-start.1) | collective-permute-done | bytes 720928 | tf_op jit(solution)/shard_map/ppermute | solution.py:29
  45.7 0.9 copy-done.11
  46.5 0.2 all-gather.2.cloned.1.call-done
  46.8 10.8 %convolution_convert_fusion.1 = bf16[2048,1408]{1,0:T(8,128)(2,1)} fusion(bf16[1024,2048]{1,0:T(8,128)(2,1)} %all-gather.2.cloned.1.call-done, bf16[1024,1408]{1,0:T(8,128)(2,1)S(1)} %add_convert_fusion.1), kind=kOutput, calls=%fused_computation.4 | convolution fusion | flops 5908463616 | bytes 12845056 | tf_op jit(solution)/shard_map/dot_general | solution.py:8
  57.7 0.2 reduce-scatter.8.cloned.1.call-start
  57.9 1.6 copy-done.3
  59.4 12.2 %convolution_convert_fusion = bf16[2048,1408]{1,0:T(8,128)(2,1)} fusion(bf16[1024,2048]{1,0:T(8,128)(2,1)} %all-gather.2.cloned.1.call-done, bf16[1024,1408]{1,0:T(8,128)(2,1)S(1)} %copy-done.3, f32[1024,1408]{1,0:T(8,128)} %get-tuple-element.23), kind=kOutput, calls=%fused_computation.3 | convolution fusion | flops 5924323328 | bytes 18612224 | tf_op jit(solution)/shard_map/dot_general | solution.py:8
  71.7 1.5 collective-permute-start.9
  73.2 0.6 collective-permute-start.4
  73.8 0.6 dynamic_slice.63
  79.7 0.7 fusion.13
  82.2 0.6 dynamic_slice.54
  87.2 0.7 fusion.12
  96.3 0.4 broadcast.44.clone
  96.7 0.7 copy-done.5
  97.4 0.1 constant_dynamic-update-slice_fusion.7
  97.5 20.8 %collective-permute-done.9 = bf16[256,1408]{1,0:T(8,128)(2,1)} collective-permute-done((bf16[256,1408]{1,0:T(8,128)(2,1)}, bf16[256,1408]{1,0:T(8,128)(2,1)}, u32[]{:S(2)}, u32[]{:S(2)}) %collective-permute-start.9) | collective-permute-done | bytes 720928 | tf_op jit(solution)/shard_map/ppermute | solution.py:29
  118.3 0.4 broadcast.44.clone.1
  118.7 0.1 constant_dynamic-update-slice_fusion.15
  118.8 2.1 collective-permute-start.5
  120.9 0.1 constant_dynamic-update-slice_fusion.6
  121.0 0.1 constant_dynamic-update-slice_fusion.14
  121.1 23.6 %collective-permute-done.10 = bf16[256,1408]{1,0:T(8,128)(2,1)S(1)} collective-permute-done((bf16[256,1408]{1,0:T(8,128)(2,1)}, bf16[256,1408]{1,0:T(8,128)(2,1)S(1)}, u32[]{:S(2)}, u32[]{:S(2)}) %collective-permute-start.10) | collective-permute-done | bytes 720928 | tf_op jit(solution)/shard_map/ppermute | solution.py:29
  144.7 1.3 constant_dynamic-update-slice_fusion.5
  146.1 2.1 collective-permute-start.6
  148.2 1.4 constant_dynamic-update-slice_fusion.4
  149.5 1.5 constant_dynamic-update-slice_fusion.12
  151.0 17.0 %collective-permute-done.11 = bf16[256,1408]{1,0:T(8,128)(2,1)S(1)} collective-permute-done((bf16[256,1408]{1,0:T(8,128)(2,1)S(1)}, bf16[256,1408]{1,0:T(8,128)(2,1)S(1)}, u32[]{:S(2)}, u32[]{:S(2)}) %collective-permute-start.11) | collective-permute-done | bytes 720928 | tf_op jit(solution)/shard_map/ppermute | solution.py:29
  168.0 2.5 collective-permute-start.12
  170.5 0.1 constant_dynamic-update-slice_fusion.3
  170.6 0.1 collective-permute-start.7
  170.7 0.1 constant_dynamic-update-slice_fusion.11
  170.8 0.1 constant_dynamic-update-slice_fusion.2
  170.9 29.6 %collective-permute-done.12 = bf16[256,1408]{1,0:T(8,128)(2,1)S(1)} collective-permute-done((bf16[256,1408]{1,0:T(8,128)(2,1)S(1)}, bf16[256,1408]{1,0:T(8,128)(2,1)S(1)}, u32[]{:S(2)}, u32[]{:S(2)}) %collective-permute-start.12) | collective-permute-done | bytes 720928 | tf_op jit(solution)/shard_map/ppermute | solution.py:29
  200.5 0.1 constant_dynamic-update-slice_fusion.10
  200.6 2.3 collective-permute-start.8
  202.9 0.1 constant_dynamic-update-slice_fusion.1
  203.0 0.1 constant_dynamic-update-slice_fusion.9
  203.1 20.8 %collective-permute-done.13 = bf16[256,1408]{1,0:T(8,128)(2,1)S(1)} collective-permute-done((bf16[256,1408]{1,0:T(8,128)(2,1)S(1)}, bf16[256,1408]{1,0:T(8,128)(2,1)S(1)}, u32[]{:S(2)}, u32[]{:S(2)}) %collective-permute-start.13) | collective-permute-done | bytes 720928 | tf_op jit(solution)/shard_map/ppermute | solution.py:29
  223.9 0.1 constant_dynamic-update-slice_fusion
  224.0 0.1 collective-permute-done.8
  224.1 0.1 constant_dynamic-update-slice_fusion.8
  224.2 10.3 %fusion.9 = f32[1024,2048]{1,0:T(8,128)} fusion(bf16[2048,1408]{1,0:T(8,128)(2,1)S(1)} %constant_dynamic-update-slice_fusion, bf16[1024,1408]{1,0:T(8,128)(2,1)S(1)} %copy-done.3, f32[1024,1408]{1,0:T(8,128)S(1)} %bitcast.40), kind=kOutput, calls=%fused_computation.46 | convolution fusion | flops 5921439744 | bytes 22806528 | tf_op jit(solution)/shard_map/dot_general | solution.py:14
  234.4 11.7 %add_convert_fusion = bf16[1024,2048]{1,0:T(8,128)(2,1)} fusion(f32[1024,2048]{1,0:T(8,128)} %fusion.9, bf16[1024,1408]{1,0:T(8,128)(2,1)} %copy-done.4, bf16[2048,1408]{1,0:T(8,128)(2,1)S(1)} %constant_dynamic-update-slice_fusion.8), kind=kOutput, calls=%fused_computation | convolution fusion | flops 5909774336 | bytes 21233664 | tf_op jit(solution)/shard_map/dot_general | solution.py:14
  246.2 2.3 collective-permute-start.14
  248.5 1.8 collective-permute-done.14
  250.3 2.1 collective-permute-start.15
  252.4 3.2 collective-permute-done.15
  255.7 2.9 collective-permute-start.16
  258.6 3.4 collective-permute-done.16
  262.0 0.6 slice_reduce_fusion
  262.6 2.3 convert_multiply_fusion.3
  264.9 74.6 %reduce-scatter.8.cloned.1.call-done = bf16[256,1408]{1,0:T(8,128)(2,1)} async-done(((bf16[2048,1408]{1,0:T(8,128)(2,1)}), bf16[256,1408]{1,0:T(8,128)(2,1)}) %reduce-scatter.8.cloned.1.call-update) | async-done | bytes 720912 | tf_op jit(solution)/shard_map/reduce_scatter | solution.py:112
  339.5 2.3 convert_multiply_fusion.2
  341.8 44.6 %reduce-scatter.4.cloned.1.call-done = bf16[256,2048]{1,0:T(8,128)(2,1)} async-done(((bf16[1024,2048]{1,0:T(8,128)(2,1)}), bf16[256,2048]{1,0:T(8,128)(2,1)}) %reduce-scatter.4.cloned.1.call-update) | async-done | bytes 1048592 | tf_op jit(solution)/shard_map/reduce_scatter | solution.py:121
  (67 shorter events, 0.5 us)
Async XLA Ops:
  7.2 6.3 %copy-start = (bf16[1024,1408]{1,0:T(8,128)(2,1)S(1)}, bf16[1024,1408]{1,0:T(8,128)(2,1)}, u32[]{:S(2)}) copy-start(bf16[1024,1408]{1,0:T(8,128)(2,1)} %param.13) | copy-start | bytes 8650756
  7.2 6.2 %copy-start.16 = (f32[3,1408]{1,0:T(4,128)S(1)}, f32[3,1408]{1,0:T(4,128)}, u32[]{:S(2)}) copy-start(f32[3,1408]{1,0:T(4,128)} %param.17) | copy-start | bytes 50692
  7.2 6.3 %copy-start.17 = (f32[1408]{0:T(1024)S(1)}, f32[1408]{0:T(1024)}, u32[]{:S(2)}) copy-start(f32[1408]{0:T(1024)} %param.18) | copy-start | bytes 16900
  7.2 39.6 %all-gather.2.cloned.1.call-start = ((), (), s32[]{:S(2)}) async-start(), calls=%async_computation.3 | async-start | bytes 5242880 | tf_op jit(solution)/shard_map/all_gather | solution.py:93
  7.9 254.7 %reduce-scatter.6.cloned.1.call-start = ((), (), s32[]{:S(2)}) async-start(), calls=%async_computation.5 | async-start | bytes 6488064 | tf_op jit(solution)/shard_map/reduce_scatter | solution.py:112
  8.0 5.5 %copy-start.1 = (bf16[1024,1408]{1,0:T(8,128)(2,1)S(1)}, bf16[1024,1408]{1,0:T(8,128)(2,1)}, u32[]{:S(2)}) copy-start(bf16[1024,1408]{1,0:T(8,128)(2,1)} %param.14) | copy-start | bytes 8650756
  8.0 5.5 %copy-start.2 = (bf16[1024,1408]{1,0:T(8,128)(2,1)S(1)}, bf16[1024,1408]{1,0:T(8,128)(2,1)}, u32[]{:S(2)}) copy-start(bf16[1024,1408]{1,0:T(8,128)(2,1)} %param.19) | copy-start | bytes 8650756
  8.0 21.3 %collective-permute-start.2 = (bf16[256,1408]{1,0:T(8,128)(2,1)}, bf16[256,1408]{1,0:T(8,128)(2,1)S(1)}, u32[]{:S(2)}, u32[]{:S(2)}) collective-permute-start(bf16[256,1408]{1,0:T(8,128)(2,1)} %param.16), channel_id=1, source_target_pairs={{4,12},{12,20},{20,28},{28,24},{24,16},{16,8},{8,0},{0,4},{5,13},{... | collective-permute-start | bytes 2162696 | tf_op jit(solution)/shard_map/ppermute | solution.py:29
  11.0 17.8 %collective-permute-start = (bf16[256,1408]{1,0:T(8,128)(2,1)}, bf16[256,1408]{1,0:T(8,128)(2,1)S(1)}, u32[]{:S(2)}, u32[]{:S(2)}) collective-permute-start(bf16[256,1408]{1,0:T(8,128)(2,1)} %param.15), channel_id=1, source_target_pairs={{0,8},{8,16},{16,24},{24,28},{28,20},{20,12},{12,4},{4,0},{1,9},{9... | collective-permute-start | bytes 2162696 | tf_op jit(solution)/shard_map/ppermute | solution.py:29
  28.8 16.9 %copy-start.9 = (bf16[256,1408]{1,0:T(8,128)(2,1)}, bf16[256,1408]{1,0:T(8,128)(2,1)S(1)}, u32[]{:S(2)}) copy-start(bf16[256,1408]{1,0:T(8,128)(2,1)S(1)} %collective-permute-done) | copy-start | bytes 2162692
  28.8 16.8 %collective-permute-start.1 = (bf16[256,1408]{1,0:T(8,128)(2,1)S(1)}, bf16[256,1408]{1,0:T(8,128)(2,1)S(1)}, u32[]{:S(2)}, u32[]{:S(2)}) collective-permute-start(bf16[256,1408]{1,0:T(8,128)(2,1)S(1)} %collective-permute-done), channel_id=1, source_target_pairs={{0,8},{8,16},{16,24},{24,28},{28,20},{20,12},{12,4},{4,0},{1,9},{9... | collective-permute-start | bytes 2162696 | tf_op jit(solution)/shard_map/ppermute | solution.py:29
  29.3 3.4 copy-start.7
  29.3 17.3 %collective-permute-start.3 = (bf16[256,1408]{1,0:T(8,128)(2,1)S(1)}, bf16[256,1408]{1,0:T(8,128)(2,1)}, u32[]{:S(2)}, u32[]{:S(2)}) collective-permute-start(bf16[256,1408]{1,0:T(8,128)(2,1)S(1)} %collective-permute-done.2), channel_id=1, source_target_pairs={{4,12},{12,20},{20,28},{28,24},{24,16},{16,8},{8,0},{0,4},{5,13},{... | collective-permute-start | bytes 2162696 | tf_op jit(solution)/shard_map/ppermute | solution.py:29
  32.7 14.1 %copy-start.4 = (bf16[1024,1408]{1,0:T(8,128)(2,1)}, bf16[1024,1408]{1,0:T(8,128)(2,1)S(1)}, u32[]{:S(2)}) copy-start(bf16[1024,1408]{1,0:T(8,128)(2,1)S(1)} %add_convert_fusion.1) | copy-start | bytes 8650756
  45.7 0.9 copy-start.11
  57.6 1.8 copy-start.3
  57.7 281.8 %reduce-scatter.8.cloned.1.call-start = ((), (), s32[]{:S(2)}) async-start(), calls=%async_computation.6 | async-start | bytes 6488064 | tf_op jit(solution)/shard_map/reduce_scatter | solution.py:112
  71.6 2.2 copy-start.19
  71.6 8.1 %copy-start.15 = (s32[8]{0:T(128)S(1)}, s32[8]{0:T(128)}, u32[]{:S(2)}) copy-start(s32[8]{0:T(128)} %constant.190.clone) | copy-start | bytes 100
  71.6 10.5 %copy-start.18 = (s32[8]{0:T(128)S(1)}, s32[8]{0:T(128)}, u32[]{:S(2)}) copy-start(s32[8]{0:T(128)} %constant.187.clone) | copy-start | bytes 100
  71.6 15.6 %copy-start.14 = (s32[8]{0:T(128)S(1)}, s32[8]{0:T(128)}, u32[]{:S(2)}) copy-start(s32[8]{0:T(128)} %constant.188.clone) | copy-start | bytes 100
  71.7 314.8 %reduce-scatter.4.cloned.1.call-start = ((), (), s32[]{:S(2)}) async-start(), calls=%async_computation.4 | async-start | bytes 5242880 | tf_op jit(solution)/shard_map/reduce_scatter | solution.py:121
  71.7 46.6 %collective-permute-start.9 = (bf16[256,1408]{1,0:T(8,128)(2,1)}, bf16[256,1408]{1,0:T(8,128)(2,1)}, u32[]{:S(2)}, u32[]{:S(2)}) collective-permute-start(bf16[256,1408]{1,0:T(8,128)(2,1)} %collective-permute-done.3), channel_id=1, source_target_pairs={{4,12},{12,20},{20,28},{28,24},{24,16},{16,8},{8,0},{0,4},{5,13},{... | collective-permute-start | bytes 2162696 | tf_op jit(solution)/shard_map/ppermute | solution.py:29
  73.2 45.6 %collective-permute-start.4 = (bf16[256,1408]{1,0:T(8,128)(2,1)}, bf16[256,1408]{1,0:T(8,128)(2,1)}, u32[]{:S(2)}, u32[]{:S(2)}) collective-permute-start(bf16[256,1408]{1,0:T(8,128)(2,1)} %copy-done.11), channel_id=1, source_target_pairs={{0,8},{8,16},{16,24},{24,28},{28,20},{20,12},{12,4},{4,0},{1,9},{9... | collective-permute-start | bytes 2162696 | tf_op jit(solution)/shard_map/ppermute | solution.py:29
  96.2 1.2 copy-start.5
  96.2 22.5 %copy-start.6 = (bf16[256,1408]{1,0:T(8,128)(2,1)S(1)}, bf16[256,1408]{1,0:T(8,128)(2,1)}, u32[]{:S(2)}) copy-start(bf16[256,1408]{1,0:T(8,128)(2,1)} %param.15) | copy-start | bytes 2162692
  97.4 23.5 %copy-start.8 = (bf16[256,1408]{1,0:T(8,128)(2,1)S(1)}, bf16[256,1408]{1,0:T(8,128)(2,1)}, u32[]{:S(2)}) copy-start(bf16[256,1408]{1,0:T(8,128)(2,1)} %copy-done.7) | copy-start | bytes 2162692
  97.4 23.6 %copy-start.10 = (bf16[256,1408]{1,0:T(8,128)(2,1)S(1)}, bf16[256,1408]{1,0:T(8,128)(2,1)}, u32[]{:S(2)}) copy-start(bf16[256,1408]{1,0:T(8,128)(2,1)} %copy-done.9) | copy-start | bytes 2162692
  97.4 47.3 %copy-start.12 = (bf16[256,1408]{1,0:T(8,128)(2,1)S(1)}, bf16[256,1408]{1,0:T(8,128)(2,1)}, u32[]{:S(2)}) copy-start(bf16[256,1408]{1,0:T(8,128)(2,1)} %copy-done.11) | copy-start | bytes 2162692
  118.3 26.4 %collective-permute-start.10 = (bf16[256,1408]{1,0:T(8,128)(2,1)}, bf16[256,1408]{1,0:T(8,128)(2,1)S(1)}, u32[]{:S(2)}, u32[]{:S(2)}) collective-permute-start(bf16[256,1408]{1,0:T(8,128)(2,1)} %collective-permute-done.9), channel_id=1, source_target_pairs={{4,12},{12,20},{20,28},{28,24},{24,16},{16,8},{8,0},{0,4},{5,13},{... | collective-permute-start | bytes 2162696 | tf_op jit(solution)/shard_map/ppermute | solution.py:29
  118.8 27.2 %collective-permute-start.5 = (bf16[256,1408]{1,0:T(8,128)(2,1)}, bf16[256,1408]{1,0:T(8,128)(2,1)S(1)}, u32[]{:S(2)}, u32[]{:S(2)}) collective-permute-start(bf16[256,1408]{1,0:T(8,128)(2,1)} %collective-permute-done.4), channel_id=1, source_target_pairs={{0,8},{8,16},{16,24},{24,28},{28,20},{20,12},{12,4},{4,0},{1,9},{9... | collective-permute-start | bytes 2162696 | tf_op jit(solution)/shard_map/ppermute | solution.py:29
  144.7 23.3 %collective-permute-start.11 = (bf16[256,1408]{1,0:T(8,128)(2,1)S(1)}, bf16[256,1408]{1,0:T(8,128)(2,1)S(1)}, u32[]{:S(2)}, u32[]{:S(2)}) collective-permute-start(bf16[256,1408]{1,0:T(8,128)(2,1)S(1)} %collective-permute-done.10), channel_id=1, source_target_pairs={{4,12},{12,20},{20,28},{28,24},{24,16},{16,8},{8,0},{0,4},{5,13},{... | collective-permute-start | bytes 2162696 | tf_op jit(solution)/shard_map/ppermute | solution.py:29
  146.1 24.6 %collective-permute-start.6 = (bf16[256,1408]{1,0:T(8,128)(2,1)S(1)}, bf16[256,1408]{1,0:T(8,128)(2,1)S(1)}, u32[]{:S(2)}, u32[]{:S(2)}) collective-permute-start(bf16[256,1408]{1,0:T(8,128)(2,1)S(1)} %collective-permute-done.5), channel_id=1, source_target_pairs={{0,8},{8,16},{16,24},{24,28},{28,20},{20,12},{12,4},{4,0},{1,9},{9... | collective-permute-start | bytes 2162696 | tf_op jit(solution)/shard_map/ppermute | solution.py:29
  148.2 76.0 %slice-start = ((s8[5767168]{0:T(1024)(128)(4,1)}), s8[4194304]{0:T(1024)(128)(4,1)S(1)}, s32[]{:S(2)}) async-start(s8[5767168]{0:T(1024)(128)(4,1)} %bitcast.39), calls=%async_computation.7 | async-start | bytes 8388608
  168.0 32.4 %collective-permute-start.12 = (bf16[256,1408]{1,0:T(8,128)(2,1)S(1)}, bf16[256,1408]{1,0:T(8,128)(2,1)S(1)}, u32[]{:S(2)}, u32[]{:S(2)}) collective-permute-start(bf16[256,1408]{1,0:T(8,128)(2,1)S(1)} %collective-permute-done.11), channel_id=1, source_target_pairs={{4,12},{12,20},{20,28},{28,24},{24,16},{16,8},{8,0},{0,4},{5,13},{... | collective-permute-start | bytes 2162696 | tf_op jit(solution)/shard_map/ppermute | solution.py:29
  170.6 29.9 %collective-permute-start.7 = (bf16[256,1408]{1,0:T(8,128)(2,1)S(1)}, bf16[256,1408]{1,0:T(8,128)(2,1)S(1)}, u32[]{:S(2)}, u32[]{:S(2)}) collective-permute-start(bf16[256,1408]{1,0:T(8,128)(2,1)S(1)} %collective-permute-done.6), channel_id=1, source_target_pairs={{0,8},{8,16},{16,24},{24,28},{28,20},{20,12},{12,4},{4,0},{1,9},{9... | collective-permute-start | bytes 2162696 | tf_op jit(solution)/shard_map/ppermute | solution.py:29
  170.8 53.4 %slice-start.1 = ((s8[5767168]{0:T(1024)(128)(4,1)}), s8[1572864]{0:T(1024)(128)(4,1)S(1)}, s32[]{:S(2)}) async-start(s8[5767168]{0:T(1024)(128)(4,1)} %bitcast.39), calls=%async_computation.8 | async-start | bytes 3145728
  200.5 23.4 %collective-permute-start.13 = (bf16[256,1408]{1,0:T(8,128)(2,1)S(1)}, bf16[256,1408]{1,0:T(8,128)(2,1)S(1)}, u32[]{:S(2)}, u32[]{:S(2)}) collective-permute-start(bf16[256,1408]{1,0:T(8,128)(2,1)S(1)} %collective-permute-done.12), channel_id=1, source_target_pairs={{4,12},{12,20},{20,28},{28,24},{24,16},{16,8},{8,0},{0,4},{5,13},{... | collective-permute-start | bytes 2162696 | tf_op jit(solution)/shard_map/ppermute | solution.py:29
  200.6 23.5 %collective-permute-start.8 = (bf16[256,1408]{1,0:T(8,128)(2,1)S(1)}, bf16[256,1408]{1,0:T(8,128)(2,1)S(1)}, u32[]{:S(2)}, u32[]{:S(2)}) collective-permute-start(bf16[256,1408]{1,0:T(8,128)(2,1)S(1)} %collective-permute-done.7), channel_id=1, source_target_pairs={{0,8},{8,16},{16,24},{24,28},{28,20},{20,12},{12,4},{4,0},{1,9},{9... | collective-permute-start | bytes 2162696 | tf_op jit(solution)/shard_map/ppermute | solution.py:29
  246.2 4.1 %collective-permute-start.14 = (f32[4,1408]{1,0:T(4,128)S(1)}, f32[4,1408]{1,0:T(4,128)S(1)}, u32[]{:S(2)}, u32[]{:S(2)}) collective-permute-start(f32[4,1408]{1,0:T(4,128)S(1)} %pad_maximum_fusion), channel_id=1, source_target_pairs={{0,4},{4,0},{8,12},{12,8},{16,20},{20,16},{24,28},{28,24},{1,5},{5... | collective-permute-start | bytes 67592 | tf_op jit(solution)/shard_map/ppermute | solution.py:55
  250.3 5.3 %collective-permute-start.15 = (f32[4,1408]{1,0:T(4,128)S(1)}, f32[4,1408]{1,0:T(4,128)S(1)}, u32[]{:S(2)}, u32[]{:S(2)}) collective-permute-start(f32[4,1408]{1,0:T(4,128)S(1)} %fusion.7), channel_id=1, source_target_pairs={{0,8},{4,12},{8,0},{12,4},{16,24},{20,28},{24,16},{28,20},{1,9},{5... | collective-permute-start | bytes 67592 | tf_op jit(solution)/shard_map/ppermute | solution.py:55
  255.7 6.3 %collective-permute-start.16 = (f32[4,1408]{1,0:T(4,128)S(1)}, f32[4,1408]{1,0:T(4,128)S(1)}, u32[]{:S(2)}, u32[]{:S(2)}) collective-permute-start(f32[4,1408]{1,0:T(4,128)S(1)} %fusion.20), channel_id=1, source_target_pairs={{0,16},{4,20},{8,24},{12,28},{16,0},{20,4},{24,8},{28,12},{1,17},{... | collective-permute-start | bytes 67592 | tf_op jit(solution)/shard_map/ppermute | solution.py:55
  262.0 124.4 %copy-start.13 = (f32[4,1408]{1,0:T(4,128)}, f32[4,1408]{1,0:T(4,128)S(1)}, u32[]{:S(2)}) copy-start(f32[4,1408]{1,0:T(4,128)S(1)} %add_multiply_fusion) | copy-start | bytes 67588
Sparse Core Ops, SparseCore 0:
  9.6 37.1 all-gather.1
  57.8 163.4 reduce-scatter.5
  224.9 114.5 reduce-scatter.7
  342.5 43.9 reduce-scatter.3
where the time goes:
time: 394 us; the launch traced here: 393 us
  waiting for transfers between devices  259 us (66%)
  matrix products  45 us (11%)
  between operations  34.1 us (9%)
  starting transfers between devices  23.9 us (6%)
  other arithmetic  18.1 us (5%)
  local copies, waits for them, and re-layouts  12.5 us (3%)
    ppermute x14, waiting for transfers between devices, ring_hops(): blocks = [*blocks, lax.ppermute(blocks[-1], axis, hops)]  131 us
    reduce_scatter x2, waiting for transfers between devices, on_device(): lax.psum_scatter(term, 'fs', scatter_dimension=0, tiled=True)  74.6 us
    reduce_scatter x1, waiting for transfers between devices, on_device(): lax.psum_scatter((contract_cols(gate_grad, full_gate) + contract_cols(val...  44.6 us
    dot_general x2, matrix products, contract_rows(): lax.dot_general(left, right, (((0,), (0,)), ((), ())), preferred_element_...  23 us
    dot_general x2, matrix products, contract_cols(): lax.dot_general(left, right, (((1,), (1,)), ((), ())), preferred_element_...  21.9 us
    ppermute x14, starting transfers between devices, ring_hops(): blocks = [*blocks, lax.ppermute(blocks[-1], axis, hops)]  16.3 us
    reduce_sum x1, other arithmetic, on_device(): jnp.sum(conv_grad * padded[:length], axis=0)  9.32 us
    ppermute x3, waiting for transfers between devices, sum_over(): lax.ppermute(terms, axis, [(i, i ^ reach) for i in range(count)])  8.42 us
  transfers between devices with their start and end apart: 21, of which 14 were waited for; matrix products, arithmetic and copies ran while one was open for 16% of the time, Pallas kernels for 0%

commit v1 on v0

v1 whole, which is shorter than its diff:
```python
import functools
import math

import jax
import jax.numpy as jnp
from jax import lax
from jax.experimental import pallas as pl
from jax.experimental.pallas import tpu as pltpu
from jax.sharding import PartitionSpec as P

MESH = pl.DeviceIdType.MESH
F32, BF16 = jnp.float32, jnp.bfloat16
PAD = 16
LANES = 128


def dot_rows(left, right):
    return lax.dot_general(left, right, (((1,), (0,)), ((), ())), preferred_element_type=F32)


def dot_cols(left, right):
    return lax.dot_general(left, right, (((1,), (1,)), ((), ())), preferred_element_type=F32)


def tiles(width, tile, body):
    whole = width // tile

    @pl.loop(0, whole)
    def _(n):
        body(pl.multiple_of(n * tile, tile), tile)

    if width % tile:
        body(whole * tile, width % tile)


def kernel(
    line, n_tp, scale,
    tok_hbm, gate_hbm, value_hbm, wg_hbm, wv_hbm, hid_hbm, taps, bias,
    ig_out, gate_out, value_out, conv_out,
    wg, wv, tok, tok_t, gst, hst, vst, cgs, acc, vfin, gfin,
    sb, sa, pair_in, vx_out, vx_in, ig_send, ig_recv, ig_sum, conv_recv, csum,
    load_sem, tok_ss, tok_rs,
    gu, gd, gx, rg, vu, vd, vx, rv,
    bu, bd, bru, brd, au, ad, aru, ard, qs, qr, xs, xr, ig_ss, ig_rs, cs, cr,
):
    me, tp = lax.axis_index("fs"), lax.axis_index("tp")
    i, j = me // 2, me % 2
    other = 2 * i + 1 - j
    up, down = me + 2, me - 2
    has_up, has_down = i < line - 1, i > 0
    n_fs = 2 * line
    rows = hid_hbm.shape[0]
    cols = hid_hbm.shape[1]
    shard = wg_hbm.shape[0]
    own_tok = tok_hbm.shape[0]
    width = tok_hbm.shape[1]
    rounds = n_fs.bit_length() - 1

    def remote(src, dst, ss, rs, fs=None, to_tp=None):
        where = {"fs": me if fs is None else fs, "tp": tp if to_tp is None else to_tp}
        return pltpu.make_async_remote_copy(
            src_ref=src, dst_ref=dst, send_sem=ss, recv_sem=rs, device_id=where, device_id_type=MESH
        )

    def gate_up(o, src):
        return remote(src, wg.at[o], gu.at[o // 2], rg.at[o], up)

    def gate_down(o, src):
        return remote(src, wg.at[o], gd.at[o // 2], rg.at[o], down)

    def gate_pair(o, src):
        return remote(src, wg.at[o], gx.at[o // 2], rg.at[o], other)

    def value_up(o, src):
        return remote(src, wv.at[o], vu.at[o], rv.at[o], up)

    def value_down(o, src):
        return remote(src, wv.at[o], vd.at[o], rv.at[o], down)

    def value_pair(src):
        return remote(src, wv.at[me], vx, rv.at[me], other)

    loads = [
        pltpu.make_async_copy(tok_hbm, tok, load_sem.at[0]),
        pltpu.make_async_copy(gate_hbm, gst.at[pl.ds(PAD, rows)], load_sem.at[1]),
        pltpu.make_async_copy(hid_hbm, hst, load_sem.at[2]),
        pltpu.make_async_copy(value_hbm, vst.at[pl.ds(0, rows)], load_sem.at[3]),
        pltpu.make_async_copy(wg_hbm, wg.at[me], load_sem.at[4]),
        pltpu.make_async_copy(wv_hbm, wv.at[me], load_sem.at[5]),
    ]
    value_pair(wv_hbm).start()
    gate_pair(me, wg_hbm).start()

    @pl.when(has_up)
    def _():
        gate_up(me, wg_hbm).start()
        value_up(me, wv_hbm).start()

    @pl.when(has_down)
    def _():
        gate_down(me, wg_hbm).start()
        value_down(me, wv_hbm).start()

    for load in loads:
        load.start()

    loads[0].wait()
    turn = 256

    @pl.loop(0, width // turn)
    def _(n):
        at = pl.multiple_of(n * turn, turn)
        tok_t[pl.ds(at, turn), pl.ds(pl.multiple_of(tp * own_tok, own_tok), own_tok)] = tok[
            :, pl.ds(at, turn)
        ].T

    def tok_piece(d, source):
        return tok_t.at[
            pl.ds(pl.multiple_of(d * 2 * shard, 2 * shard), 2 * shard),
            pl.ds(pl.multiple_of(source * own_tok, own_tok), own_tok),
        ]

    def far(n):
        return jnp.where(n % 2 == 0, line - 1 - n // 2, n // 2)

    def tok_copy(d, step):
        peer = (tp + step) % n_tp
        return remote(tok_piece(d, tp), tok_piece(d, tp), tok_ss.at[step, d], tok_rs.at[tp, d], to_tp=peer)

    def tok_landed(d):
        @pl.loop(1, n_tp)
        def _(step):
            source = (tp + step) % n_tp
            remote(tok_piece(d, source), tok_piece(d, source), tok_ss.at[0, d], tok_rs.at[source, d]).wait_recv()

    @pl.loop(0, line)
    def _(n):
        @pl.loop(1, n_tp)
        def _(step):
            tok_copy(far(n), step).start()

    loads[1].wait()
    loads[2].wait()
    loads[3].wait()
    chunk = 64
    root = math.sqrt(2.0 / math.pi)

    def elementwise(at, size):
        cut = pl.ds(at, size)
        gst[pl.ds(0, PAD), cut] = jnp.zeros((PAD, size), BF16)
        w0, w1, w2 = (taps[pl.ds(k, 1), cut] for k in range(3))
        b = bias[:, cut]

        def forward(n, sums):
            r = pl.multiple_of(n * chunk, chunk)
            wide = gst[pl.ds(r, PAD + chunk), cut].astype(F32)
            x0 = wide[PAD:]
            x1 = pltpu.roll(wide, 1, 0)[PAD:]
            x2 = pltpu.roll(wide, 2, 0)[PAD:]
            z = b + w0 * x2 + w1 * x1 + w2 * x0
            sq = z * z
            th = jnp.tanh(root * (z + 0.044715 * (sq * z)))
            cdf = 0.5 * (1.0 + th)
            h = hst[pl.ds(r, chunk), cut].astype(F32)
            v = vst[pl.ds(r, chunk), cut].astype(F32)
            hst[pl.ds(r, chunk), cut] = (h * (z * cdf)).astype(BF16)
            slope = cdf + (0.5 * z) * (1.0 - th * th) * (root + (3.0 * 0.044715 * root) * sq)
            cg = slope * (h * v)
            cgs[pl.ds(r, chunk), pl.ds(0, size)] = cg

            def fold(term):
                return jnp.sum(term.reshape(chunk // 8, 8, size), axis=0)

            return tuple(s + fold(t) for s, t in zip(sums, (cg * x2, cg * x1, cg * x0, cg)))

        zero = jnp.zeros((8, size), F32)
        sums = lax.fori_loop(0, rows // chunk, forward, (zero,) * 4)
        for k in range(4):
            csum[pl.ds(k, 1), cut] = jnp.sum(sums[k], axis=0, keepdims=True)
        cgs[pl.ds(rows, 8), pl.ds(0, size)] = jnp.zeros((8, size), F32)

        @pl.loop(0, rows // chunk)
        def _(n):
            r = pl.multiple_of(n * chunk, chunk)
            wide = cgs[pl.ds(r, chunk + 8), pl.ds(0, size)]
            g1 = pltpu.roll(wide, chunk + 7, 0)[:chunk]
            g2 = pltpu.roll(wide, chunk + 6, 0)[:chunk]
            gst[pl.ds(PAD + r, chunk), cut] = (w2 * wide[:chunk] + w1 * g1 + w0 * g2).astype(BF16)

    tiles(cols, LANES, elementwise)

    def conv_copy(r):
        return remote(csum.at[pl.ds(0, 4)], conv_recv.at[r], cs.at[r], cr.at[r], me ^ (1 << r))

    def conv_add(r):
        conv_copy(r).wait_send()
        conv_copy(r).wait_recv()
        csum[pl.ds(0, 4), :] += conv_recv[r]

    conv_copy(0).start()

    remote(wv.at[other], wv.at[other], vx, rv.at[other]).wait_recv()

    @pl.when(has_up)
    def _():
        value_up(other, wv.at[other]).start()

    @pl.when(has_down)
    def _():
        value_down(other, wv.at[other]).start()

    def gather(t):
        low, high = i - t - 1, i + t + 1

        @pl.when(low >= 0)
        def _():
            o = 2 * low + j
            gate_up(o, wg.at[o]).wait_recv()

            @pl.when(has_up)
            def _():
                gate_up(o, wg.at[o]).start()

            gate_pair(o, wg.at[o]).start()

        @pl.when(high < line)
        def _():
            o = 2 * high + j
            gate_down(o, wg.at[o]).wait_recv()

            @pl.when(has_down)
            def _():
                gate_down(o, wg.at[o]).start()

            gate_pair(o, wg.at[o]).start()

        for flip in range(2):
            jd = j if flip == 0 else 1 - j

            @pl.when(low >= 0)
            def _():
                o = 2 * low + jd
                value_up(o, wv.at[o]).wait_recv()

                @pl.when(has_up)
                def _():
                    value_up(o, wv.at[o]).start()

            @pl.when(high < line)
            def _():
                o = 2 * high + jd
                value_down(o, wv.at[o]).wait_recv()

                @pl.when(has_down)
                def _():
                    value_down(o, wv.at[o]).start()

    def gate_grad(cut):
        return gst[pl.ds(PAD, rows), cut]

    def value_grad(cut):
        return hst[:, cut]

    def term(grad, o):
        left = pl.ds(pl.multiple_of(o * shard, shard), shard)

        def one(at, size):
            cut = pl.ds(at, size)
            acc[:, cut] = dot_rows(tok_t[left, :], grad(cut))

        tiles(cols, 256, one)

    step_rows = 16

    def each_rows(body):
        @pl.loop(0, shard // step_rows)
        def _(n):
            body(pl.ds(pl.multiple_of(n * step_rows, step_rows), step_rows))

    def put(dst, *more):
        def body(cut):
            total = acc[cut, :]
            for ref in more:
                total = total + ref[cut, :].astype(F32)
            dst[cut, :] = total.astype(dst.dtype)

        each_rows(body)

    def landing(d, receiver):
        return jnp.where(d == receiver, line, d)

    def hop(grad, slots, o, d, going_up, ss, rs, extra=None):
        term(grad, o)
        more = () if extra is None else (extra(),)
        slot = slots.at[d]
        came = has_down if going_up else has_up
        if going_up:
            arrived = remote(slot, slot, ss, rs)
            sent = remote(slot, slot, ss, rs, up)
        else:
            arrived = remote(slot, slot, ss, rs)
            sent = remote(slot, slots.at[landing(d, i - 1)], ss, rs, down)

        @pl.when(came)
        def _():
            arrived.wait_recv()
            put(slot, slot, *more)

        @pl.when(jnp.logical_not(came))
        def _():
            put(slot, *more)

        sent.start()

    def up_row(tt):
        return line - 1 - tt + i

    def down_row(tt):
        return tt - line + 1 + i

    def value_step(tt):
        for jd in range(2):
            @pl.when(tt >= i)
            def _():
                d = up_row(tt)
                hop(value_grad, sb.at[jd], 2 * d + jd, d, True, bu.at[jd, d], bru.at[jd, d])

            @pl.when(tt >= line - 1 - i)
            def _():
                d = down_row(tt)
                hop(value_grad, sb.at[jd], 2 * d + jd, d, False, bd.at[jd, d], brd.at[jd, d])

    def pair_copy(d):
        return remote(vst.at[pl.ds(pl.multiple_of(d * shard, shard), shard)], pair_in.at[d], qs.at[d], qr.at[d], other)

    def pair_term(n):
        d = far(n)
        term(gate_grad, 2 * d + 1 - j)
        put(vst.at[pl.ds(pl.multiple_of(d * shard, shard), shard)])
        pair_copy(d).start()

    def from_pair(d):
        def get():
            pair_copy(d).wait_recv()
            return pair_in.at[d]

        return get

    def gate_step(tt):
        @pl.when(tt >= i)
        def _():
            d = up_row(tt)
            hop(gate_grad, sa, 2 * d + j, d, True, au.at[d], aru.at[d], from_pair(d))

        @pl.when(tt >= line - 1 - i)
        def _():
            d = down_row(tt)
            hop(gate_grad, sa, 2 * d + j, d, False, ad.at[d], ard.at[d], from_pair(d))

    def share_copy(k, o):
        return remote(ig_send.at[k, o], ig_recv.at[tp, o], ig_ss.at[k, o], ig_rs.at[tp, o], to_tp=k)

    def share(o):
        @pl.loop(0, n_tp)
        def _(k):
            at = pl.multiple_of(k * own_tok, own_tok)
            part = dot_cols(gst[pl.ds(PAD + at, own_tok), :], wg[o]) + dot_cols(hst[pl.ds(at, own_tok), :], wv[o])
            ig_send[k, o] = part.astype(BF16)

            @pl.when(k != tp)
            def _():
                share_copy(k, o).start()

    def share_line(t):
        for at in (i - t, i + t):
            @pl.when((at >= 0) & (at < line))
            def _():
                share(2 * at + j)

    def share_pair(t, both=True):
        for at in (i - t, i + t)[: 2 if both else 1]:
            @pl.when((at >= 0) & (at < line))
            def _():
                o = 2 * at + 1 - j
                gate_pair(o, wg.at[o]).wait_recv()
                share(o)

    loads[4].wait()
    loads[5].wait()

    @pl.loop(0, line)
    def _(n):
        tok_landed(far(n))

    pair_term(0)
    value_step(0)
    share(me)

    @pl.loop(1, line - 1)
    def _(tt):
        gather(tt - 1)
        pair_term(tt)

        @pl.when(tt < rounds)
        def _():
            conv_add(tt - 1)
            conv_copy(tt).start()

        value_step(tt)
        share_line(tt)

        @pl.when(tt == 1)
        def _():
            share_pair(0, False)

        @pl.when(tt > 1)
        def _():
            share_pair(tt - 1)

    gather(line - 2)
    pair_term(line - 1)
    conv_add(rounds - 1)
    share_line(line - 1)

    gate_step(0)
    share_pair(line - 2)

    @pl.loop(1, line - 1)
    def _(tt):
        gate_step(tt)

    def arrive(slots, ru, rd):
        @pl.when(has_down)
        def _():
            remote(slots.at[i], slots.at[i], xs, ru.at[i]).wait_recv()
            put(acc, slots.at[i])

        @pl.when(has_up)
        def _():
            remote(slots.at[line], slots.at[line], xs, rd.at[i]).wait_recv()
            put(acc, slots.at[line])

    term(value_grad, other)
    arrive(sb.at[1 - j], bru.at[1 - j], brd.at[1 - j])
    put(vx_out)
    cross = remote(vx_out, vx_in, xs, xr, other)
    cross.start()
    term(value_grad, me)
    arrive(sb.at[j], bru.at[j], brd.at[j])
    put(vfin)
    share_pair(line - 1)

    term(gate_grad, me)
    put(acc, from_pair(i)())
    arrive(sa, aru, ard)

    def finish_gate(cut):
        gfin[cut, :] = acc[cut, :] * scale

    each_rows(finish_gate)
    store_gate = pltpu.make_async_copy(gfin, gate_out, load_sem.at[0])
    store_gate.start()
    cross.wait_recv()

    def finish_value(cut):
        vfin[cut, :] = (vfin[cut, :] + vx_in[cut, :].astype(F32)) * scale

    each_rows(finish_value)
    store_value = pltpu.make_async_copy(vfin, value_out, load_sem.at[1])
    store_value.start()

    conv_out[...] = csum[pl.ds(0, 4), :] * scale

    @pl.loop(0, n_fs)
    def _(o):
        @pl.loop(1, n_tp)
        def _(step):
            source = (tp + step) % n_tp
            remote(ig_send.at[source, o], ig_recv.at[source, o], ig_ss.at[source, o], ig_rs.at[source, o]).wait_recv()

    for o in range(n_fs):
        total = ig_send[tp, o].astype(F32)
        for step in range(1, n_tp):
            total = total + ig_recv[(tp + step) % n_tp, o].astype(F32)
        ig_sum[:, o * shard : (o + 1) * shard] = total.astype(BF16)
    store_input = pltpu.make_async_copy(ig_sum, ig_out, load_sem.at[2])
    store_input.start()

    value_pair(wv_hbm).wait_send()
    cross.wait_send()

    @pl.loop(0, line)
    def _(d):
        @pl.loop(1, n_tp)
        def _(step):
            tok_copy(d, step).wait_send()

        pair_copy(d).wait_send()
        gate_pair(2 * d, wg_hbm).wait_send()

        @pl.when(has_up & (d <= i))
        def _():
            gate_up(2 * d, wg_hbm).wait_send()
            value_up(2 * d, wv_hbm).wait_send()
            value_up(2 * d + 1, wv_hbm).wait_send()

        @pl.when(has_down & (d >= i))
        def _():
            gate_down(2 * d, wg_hbm).wait_send()
            value_down(2 * d, wv_hbm).wait_send()
            value_down(2 * d + 1, wv_hbm).wait_send()

        @pl.when(d > i)
        def _():
            for jd in range(2):
                remote(sb.at[jd, d], sb.at[jd, d], bu.at[jd, d], bru.at[jd, d]).wait_send()
            remote(sa.at[d], sa.at[d], au.at[d], aru.at[d]).wait_send()

        @pl.when(d < i)
        def _():
            for jd in range(2):
                remote(sb.at[jd, d], sb.at[jd, d], bd.at[jd, d], brd.at[jd, d]).wait_send()
            remote(sa.at[d], sa.at[d], ad.at[d], ard.at[d]).wait_send()

    @pl.loop(0, n_fs)
    def _(o):
        @pl.loop(1, n_tp)
        def _(step):
            share_copy((tp + step) % n_tp, o).wait_send()

    store_gate.wait()
    store_value.wait()
    store_input.wait()


def on_device(
    tokens, gate_pre, value_pre, up_gate_w, up_value_w, conv_weight, conv_bias, hidden_grad
):
    n_fs, n_tp = lax.axis_size("fs"), lax.axis_size("tp")
    line = n_fs // 2
    rows, cols = gate_pre.shape
    own_tok, width = tokens.shape
    shard = up_gate_w.shape[0]
    rounds = n_fs.bit_length() - 1
    assert n_fs == 1 << rounds and line >= rounds + 1 and shard * n_fs == width
    scale = float(rows * n_fs) ** (-0.5)
    any_space = pl.BlockSpec(memory_space=pl.ANY)
    vmem = pl.BlockSpec(memory_space=pltpu.VMEM)
    dma = pltpu.SemaphoreType.DMA
    block = (shard, cols)
    input_grad, gate_out, value_out, conv = pl.pallas_call(
        functools.partial(kernel, line, n_tp, scale),
        out_shape=(
            jax.ShapeDtypeStruct((own_tok, width), BF16),
            jax.ShapeDtypeStruct(block, F32),
            jax.ShapeDtypeStruct(block, F32),
            jax.ShapeDtypeStruct((4, cols), F32),
        ),
        in_specs=[any_space] * 6 + [vmem] * 2,
        out_specs=(any_space, any_space, any_space, vmem),
        scratch_shapes=[
            pltpu.VMEM((n_fs, *block), BF16),
            pltpu.VMEM((n_fs, *block), BF16),
            pltpu.VMEM((own_tok, width), BF16),
            pltpu.VMEM((width, rows), BF16),
            pltpu.VMEM((PAD + rows, cols), BF16),
            pltpu.VMEM((rows, cols), BF16),
            pltpu.VMEM((max(rows, line * shard), cols), BF16),
            pltpu.VMEM((rows + 8, LANES), F32),
            pltpu.VMEM(block, F32),
            pltpu.VMEM(block, F32),
            pltpu.VMEM(block, F32),
            pltpu.VMEM((2, line + 1, *block), BF16),
            pltpu.VMEM((line + 1, *block), BF16),
            pltpu.VMEM((line, *block), BF16),
            pltpu.VMEM(block, BF16),
            pltpu.VMEM(block, BF16),
            pltpu.VMEM((n_tp, n_fs, own_tok, shard), BF16),
            pltpu.VMEM((n_tp, n_fs, own_tok, shard), BF16),
            pltpu.VMEM((own_tok, width), BF16),
            pltpu.VMEM((rounds, 4, cols), F32),
            pltpu.VMEM((8, cols), F32),
            dma((6,)),
            dma((n_tp, line)),
            dma((n_tp, line)),
            *[dma((line,))] * 3,
            dma((n_fs,)),
            dma((n_fs,)),
            dma((n_fs,)),
            dma,
            dma((n_fs,)),
            *[dma((2, line))] * 4,
            *[dma((line,))] * 4,
            *[dma((line,))] * 2,
            dma,
            dma,
            *[dma((n_tp, n_fs))] * 2,
            *[dma((rounds,))] * 2,
        ],
        compiler_params=pltpu.CompilerParams(has_side_effects=True, vmem_limit_bytes=67_000_000),
        name="backward",
    )(
        tokens, gate_pre, value_pre, up_gate_w, up_value_w, hidden_grad,
        conv_weight, conv_bias.reshape(1, cols),
    )
    return (input_grad, gate_out, value_out, conv[:3], conv[3])


def solution(mesh):
    return jax.shard_map(
        on_device,
        mesh=mesh,
        in_specs=(
            P(("fs", "tp"), None),
            P("fs", "tp"),
            P("fs", "tp"),
            P("fs", "tp"),
            P("fs", "tp"),
            P(None, "tp"),
            P("tp"),
            P("fs", "tp"),
        ),
        out_specs=(P(("fs", "tp"), None), P("fs", "tp"), P("fs", "tp"), P(None, "tp"), P("tp")),
        check_vma=False,
    )
```

time: 394 us -> 225 us (0.57)
  the two profiles are of different devices: /device:TPU:0 before, /device:TPU:17 now
where the time goes in v1:
time: 225 us
  Pallas kernels  216 us (96%)
  local copies, waits for them, and re-layouts  8.66 us (4%)
    pallas_call x1, Pallas kernels, on_device(): pl.pallas_call(functools.partial(kernel, line, n_tp, scale), out_shape=(j...  216 us
    unnamed x10, local copies, waits for them, and re-layouts  5.9 us

profile of v1, /device:TPU:17, one launch (start us, length us, event | category | flops | bytes accessed | tf_op | source)
XLA Modules:
  0.0 224.9 jit_solution(8918673351320583122)
XLA Ops:
  0.6 1.3 reshape.13.bias
  1.9 215.6 %backward.1 = (bf16[256,2048]{1,0:T(8,128)(2,1)}, f32[256,1408]{1,0:T(8,128)}, f32[256,1408]{1,0:T(8,128)}, f32[4,1408]{1,0:T(4,128)}) custom-call(bf16[256,2048]{1,0:T(8,128)(2,1)} %tok_hbm.1, bf16[1024,1408]{1,0:T(8,128)(2,1)} %gate_hbm.1, bf16[1024,1408]{1,0:T(8,128)(2,1)} %value_hbm.1, bf16[256,1408]{1,0:T(8,128)(2,1)} %wg_hbm.1, ...), custom_call_target="tpu_custom_call" | custom-call | tf_op jit(solution)/shard_map/backward/pallas_call | solution.py:551
  217.5 0.0 copy-start.1
  217.5 1.5 slice_reduce_fusion
  219.0 2.3 %copy.17 = bf16[256,2048]{1,0:T(8,128)(2,1)} copy(bf16[256,2048]{1,0:T(8,128)(2,1)} %get-tuple-element.18) | data formatting | bytes 2097152
  221.3 0.0 copy-done.1
  221.3 0.0 copy-start
  221.3 1.1 copy.18
  222.4 0.8 copy-done
  223.1 0.0 copy-start.2
  223.1 1.1 copy.19
  224.2 0.0 copy-done.2
  224.3 0.6 copy.20
Async XLA Ops:
  217.5 3.8 %copy-start.1 = (f32[256,1408]{1,0:T(8,128)S(1)}, f32[256,1408]{1,0:T(8,128)}, u32[]{:S(2)}) copy-start(f32[256,1408]{1,0:T(8,128)} %get-tuple-element.19) | copy-start | bytes 4325380
  221.3 1.9 copy-start
  223.1 1.1 copy-start.2

commit v2 on v1

v2 whole, which is shorter than its diff:
```python
import functools
import math

import jax
import jax.numpy as jnp
from jax import lax
from jax.experimental import pallas as pl
from jax.experimental.pallas import tpu as pltpu
from jax.sharding import PartitionSpec as P

MESH = pl.DeviceIdType.MESH
F32, BF16 = jnp.float32, jnp.bfloat16
PAD = 16
LANES = 128
SPLIT = 2


def dot_rows(left, right):
    return lax.dot_general(left, right, (((1,), (0,)), ((), ())), preferred_element_type=F32)


def dot_cols(left, right):
    return lax.dot_general(left, right, (((1,), (1,)), ((), ())), preferred_element_type=F32)


def tiles(width, tile, body):
    whole = width // tile

    @pl.loop(0, whole)
    def _(n):
        body(pl.multiple_of(n * tile, tile), tile)

    if width % tile:
        body(whole * tile, width % tile)


def kernel(
    line, n_tp, split, scale,
    tok_hbm, gate_hbm, value_hbm, wg_hbm, wv_hbm, hid_hbm, taps, bias,
    ig_sum, gfin, vfin, conv_out, bias_out,
    wa, wb, tok, tok_t, gst, hst, vst, cgs, acc,
    sb, sa, pair_in, vx_out, vx_in, ig_send, ig_recv, conv_recv, csum,
    load_sem, tok_ss, tok_relay, tok_rs,
    a_up, a_down, ax, ra, b_up, b_down, bx, rb,
    bu, bd, bru, brd, au, ad, aru, ard, qs, qr, xs, xr, ig_ss, ig_rs, cs, cr,
):
    me, tp = lax.axis_index("fs"), lax.axis_index("tp")
    i, j = me // 2, me % 2
    other = 2 * i + 1 - j
    up, down = me + 2, me - 2
    has_up, has_down = i < line - 1, i > 0
    n_fs = 2 * line
    rows = hid_hbm.shape[0]
    cols = hid_hbm.shape[1]
    shard = wg_hbm.shape[0]
    own_tok = tok_hbm.shape[0]
    width = tok_hbm.shape[1]
    rounds = n_fs.bit_length() - 1

    def remote(src, dst, ss, rs, fs=None, to_tp=None):
        where = {"fs": me if fs is None else fs, "tp": tp if to_tp is None else to_tp}
        return pltpu.make_async_remote_copy(
            src_ref=src, dst_ref=dst, send_sem=ss, recv_sem=rs, device_id=where, device_id_type=MESH
        )

    def columns_of(ref, first, count):
        return ref if count == ref.shape[-1] else ref.at[:, pl.ds(first, count)]

    barrier = pltpu.get_barrier_semaphore()

    def greet(fs, to_tp):
        pl.semaphore_signal(barrier, inc=1, device_id={"fs": fs, "tp": to_tp}, device_id_type=MESH)

    def part_a(o, ss, to):
        return remote(wa.at[o], wa.at[o], ss.at[o // 2], ra.at[o], to)

    def part_b(o, ss, to):
        return remote(wb.at[o], wb.at[o], ss.at[o], rb.at[o], to)

    def along(part, o, up_ss, down_ss, go_up, go_down):
        @pl.when(go_up)
        def _():
            part(o, up_ss, up).start()

        @pl.when(go_down)
        def _():
            part(o, down_ss, down).start()

    loads = [
        pltpu.make_async_copy(tok_hbm, tok, load_sem.at[0]),
        pltpu.make_async_copy(columns_of(wv_hbm, split, cols - split), wb.at[me], load_sem.at[1]),
        pltpu.make_async_copy(wg_hbm, columns_of(wa.at[me], split, cols), load_sem.at[2]),
        pltpu.make_async_copy(gate_hbm, gst.at[pl.ds(PAD, rows)], load_sem.at[3]),
        pltpu.make_async_copy(hid_hbm, hst, load_sem.at[4]),
        pltpu.make_async_copy(value_hbm, columns_of(vst.at[pl.ds(0, rows)], 0, cols), load_sem.at[5]),
    ]
    if split:
        loads.insert(1, pltpu.make_async_copy(
            columns_of(wv_hbm, 0, split), columns_of(wa.at[me], 0, split), load_sem.at[6]
        ))
    for load in loads:
        load.start()

    greet(other, tp)

    @pl.when(has_up)
    def _():
        greet(up, tp)

    @pl.when(has_down)
    def _():
        greet(down, tp)

    for r in range(2, rounds):
        greet(me ^ (1 << r), tp)

    @pl.loop(1, n_tp)
    def _(step):
        greet(me, (tp + step) % n_tp)

    met = 1 + (rounds - 2) + (n_tp - 1) + jnp.where(has_up, 1, 0) + jnp.where(has_down, 1, 0)
    pl.semaphore_wait(barrier, met)

    weights = 4 if split else 3
    for load in loads[1:weights]:
        load.wait()
    part_b(me, bx, other).start()
    part_a(me, ax, other).start()
    along(part_a, me, a_up, a_down, has_up, has_down)
    along(part_b, me, b_up, b_down, has_up, has_down)

    loads[0].wait()
    turn = 256

    @pl.loop(0, width // turn)
    def _(n):
        at = pl.multiple_of(n * turn, turn)
        tok_t[pl.ds(at, turn), pl.ds(pl.multiple_of(tp * own_tok, own_tok), own_tok)] = tok[
            :, pl.ds(at, turn)
        ].T

    def tok_piece(d, source):
        return tok_t.at[
            pl.ds(pl.multiple_of(d * 2 * shard, 2 * shard), 2 * shard),
            pl.ds(pl.multiple_of(source * own_tok, own_tok), own_tok),
        ]

    def far(n):
        mirror = 2 * i >= line
        at = jnp.where(mirror, line - 1 - i, i)
        d = line - 1 - n
        d = jnp.where(d > at, d, jnp.where(d == 0, at, d - 1))
        return jnp.where(mirror, line - 1 - d, d)

    def tok_copy(d, source, ss, to):
        return remote(tok_piece(d, source), tok_piece(d, source), ss, tok_rs.at[source, d], to_tp=to)

    core, twin, chips = tp % 2, tp + 1 - 2 * (tp % 2), n_tp // 2

    def on_chip(step):
        return 2 * ((tp // 2 + step) % chips) + core

    @pl.loop(0, line)
    def _(n):
        d = far(n)

        @pl.loop(1, chips)
        def _(step):
            tok_copy(d, tp, tok_ss.at[on_chip(step), d], on_chip(step)).start()

        tok_copy(d, tp, tok_relay.at[tp, d], twin).start()

    def tok_relayed(d):
        @pl.loop(1, chips)
        def _(step):
            source = on_chip(step)
            tok_copy(d, source, tok_relay.at[source, d], twin).wait_recv()
            tok_copy(d, source, tok_relay.at[source, d], twin).start()

    def tok_landed(d):
        @pl.loop(0, chips)
        def _(step):
            source = on_chip(step) + twin - tp
            tok_copy(d, source, tok_relay.at[source, d], twin).wait_recv()

    for load in loads[weights:]:
        load.wait()
    chunk = 64
    root = math.sqrt(2.0 / math.pi)

    def elementwise(at, size):
        cut = pl.ds(at, size)
        gst[pl.ds(0, PAD), cut] = jnp.zeros((PAD, size), BF16)
        w0, w1, w2 = (taps[pl.ds(k, 1), cut] for k in range(3))
        b = bias[:, cut]

        def forward(n, sums):
            r = pl.multiple_of(n * chunk, chunk)
            wide = gst[pl.ds(r, PAD + chunk), cut].astype(F32)
            x0 = wide[PAD:]
            x1 = pltpu.roll(wide, 1, 0)[PAD:]
            x2 = pltpu.roll(wide, 2, 0)[PAD:]
            z = b + w0 * x2 + w1 * x1 + w2 * x0
            sq = z * z
            th = jnp.tanh(root * (z + 0.044715 * (sq * z)))
            cdf = 0.5 * (1.0 + th)
            h = hst[pl.ds(r, chunk), cut].astype(F32)
            v = vst[pl.ds(r, chunk), cut].astype(F32)
            hst[pl.ds(r, chunk), cut] = (h * (z * cdf)).astype(BF16)
            slope = cdf + (0.5 * z) * (1.0 - th * th) * (root + (3.0 * 0.044715 * root) * sq)
            cg = slope * (h * v)
            cgs[pl.ds(r, chunk), pl.ds(0, size)] = cg

            def fold(term):
                return jnp.sum(term.reshape(chunk // 8, 8, size), axis=0)

            return tuple(s + fold(t) for s, t in zip(sums, (cg * x2, cg * x1, cg * x0, cg)))

        zero = jnp.zeros((8, size), F32)
        sums = lax.fori_loop(0, rows // chunk, forward, (zero,) * 4)
        for k in range(4):
            csum[pl.ds(k, 1), cut] = jnp.sum(sums[k], axis=0, keepdims=True)
        cgs[pl.ds(rows, 8), pl.ds(0, size)] = jnp.zeros((8, size), F32)

        @pl.loop(0, rows // chunk)
        def _(n):
            r = pl.multiple_of(n * chunk, chunk)
            wide = cgs[pl.ds(r, chunk + 8), pl.ds(0, size)]
            g1 = pltpu.roll(wide, chunk + 7, 0)[:chunk]
            g2 = pltpu.roll(wide, chunk + 6, 0)[:chunk]
            gst[pl.ds(PAD + r, chunk), cut] = (w2 * wide[:chunk] + w1 * g1 + w0 * g2).astype(BF16)

    tiles(cols, LANES, elementwise)

    def conv_copy(r):
        return remote(csum.at[pl.ds(0, 4)], conv_recv.at[r], cs.at[r], cr.at[r], me ^ (1 << r))

    def conv_add(r):
        conv_copy(r).wait_send()
        conv_copy(r).wait_recv()
        csum[pl.ds(0, 4), :] += conv_recv[r]

    conv_copy(0).start()

    part_b(other, bx, other).wait_recv()
    along(part_b, other, b_up, b_down, has_up, has_down)

    def gather(t):
        low, high = i - t - 1, i + t + 1

        @pl.when(low >= 0)
        def _():
            o = 2 * low + j
            part_a(o, a_up, up).wait_recv()
            along(part_a, o, a_up, a_down, has_up, False)
            part_a(o, ax, other).start()

        @pl.when(high < line)
        def _():
            o = 2 * high + j
            part_a(o, a_down, down).wait_recv()
            along(part_a, o, a_up, a_down, False, has_down)
            part_a(o, ax, other).start()

        for flip in range(2):
            jd = j if flip == 0 else 1 - j

            @pl.when(low >= 0)
            def _():
                o = 2 * low + jd
                part_b(o, b_up, up).wait_recv()
                along(part_b, o, b_up, b_down, has_up, False)

            @pl.when(high < line)
            def _():
                o = 2 * high + jd
                part_b(o, b_down, down).wait_recv()
                along(part_b, o, b_up, b_down, False, has_down)

    wide_a, wide_b = cols + split, cols - split

    def value_cols(at, size):
        return hst[:, pl.ds(at, size)]

    def value_rest(at, size):
        return hst[:, pl.ds(pl.multiple_of(at + split, LANES), size)]

    def gate_cols(at, size):
        return gst[pl.ds(PAD, rows), pl.ds(at, size)]

    def columns(grad, left, first, count):
        def one(at, size):
            to = pl.ds(pl.multiple_of(at + first, LANES), size)
            acc[:, to] = dot_rows(tok_t[left, :], grad(at, size))

        tiles(count, 256, one)

    def term(is_a, o):
        left = pl.ds(pl.multiple_of(o * shard, shard), shard)
        if is_a:
            if split:
                columns(value_cols, left, 0, split)
            columns(gate_cols, left, split, cols)
        else:
            columns(value_rest, left, 0, wide_b)

    step_rows = 16

    def each_rows(body):
        @pl.loop(0, shard // step_rows)
        def _(n):
            body(pl.ds(pl.multiple_of(n * step_rows, step_rows), step_rows))

    def put(dst, *more):
        span = pl.ds(0, dst.shape[-1])

        def body(cut):
            total = acc[cut, span]
            for ref in more:
                total = total + ref[cut, :].astype(F32)
            dst[cut, span] = total.astype(dst.dtype)

        each_rows(body)

    def landing(d, receiver):
        return jnp.where(d == receiver, line, d)

    def hop(is_a, slots, o, d, going_up, ss, rs, extra=None):
        term(is_a, o)
        more = () if extra is None else (extra(),)
        slot = slots.at[d]
        came = has_down if going_up else has_up
        if going_up:
            arrived = remote(slot, slot, ss, rs)
            sent = remote(slot, slot, ss, rs, up)
        else:
            arrived = remote(slot, slot, ss, rs)
            sent = remote(slot, slots.at[landing(d, i - 1)], ss, rs, down)

        @pl.when(came)
        def _():
            arrived.wait_recv()
            put(slot, slot, *more)

        @pl.when(jnp.logical_not(came))
        def _():
            put(slot, *more)

        sent.start()

    def up_row(tt):
        return line - 1 - tt + i

    def down_row(tt):
        return tt - line + 1 + i

    def value_step(tt):
        for jd in range(2):
            @pl.when(tt >= i)
            def _():
                d = up_row(tt)
                hop(False, sb.at[jd], 2 * d + jd, d, True, bu.at[jd, d], bru.at[jd, d])

            @pl.when(tt >= line - 1 - i)
            def _():
                d = down_row(tt)
                hop(False, sb.at[jd], 2 * d + jd, d, False, bd.at[jd, d], brd.at[jd, d])

    def pair_copy(d):
        return remote(vst.at[pl.ds(pl.multiple_of(d * shard, shard), shard), :], pair_in.at[d], qs.at[d], qr.at[d], other)

    def pair_term(n):
        d = far(n)
        term(True, 2 * d + 1 - j)
        put(vst.at[pl.ds(pl.multiple_of(d * shard, shard), shard), :])
        pair_copy(d).start()

    def from_pair(d):
        def get():
            pair_copy(d).wait_recv()
            return pair_in.at[d]

        return get

    def gate_step(tt):
        @pl.when(tt >= i)
        def _():
            d = up_row(tt)
            hop(True, sa, 2 * d + j, d, True, au.at[d], aru.at[d], from_pair(d))

        @pl.when(tt >= line - 1 - i)
        def _():
            d = down_row(tt)
            hop(True, sa, 2 * d + j, d, False, ad.at[d], ard.at[d], from_pair(d))

    def share_copy(k, o):
        return remote(ig_send.at[k, o], ig_recv.at[tp, o], ig_ss.at[k, o], ig_rs.at[tp, o], to_tp=k)

    def share(o):
        @pl.loop(0, n_tp)
        def _(k):
            at = pl.multiple_of(k * own_tok, own_tok)
            here = pl.ds(at, own_tok)
            part = dot_cols(gst[pl.ds(PAD + at, own_tok), :], wa[o, :, pl.ds(split, cols)])
            if split:
                part = part + dot_cols(hst[here, pl.ds(0, split)], wa[o, :, pl.ds(0, split)])
            part = part + dot_cols(hst[here, pl.ds(split, wide_b)], wb[o])
            ig_send[k, o] = part.astype(BF16)

            @pl.when(k != tp)
            def _():
                share_copy(k, o).start()

    def share_line(t):
        for at in (i - t, i + t):
            @pl.when((at >= 0) & (at < line))
            def _():
                share(2 * at + j)

    def share_pair(t, both=True):
        for at in (i - t, i + t)[: 2 if both else 1]:
            @pl.when((at >= 0) & (at < line))
            def _():
                o = 2 * at + 1 - j
                part_a(o, ax, other).wait_recv()
                share(o)

    for n in range(min(2, line)):
        tok_relayed(far(n))
    for n in range(min(2, line)):
        tok_landed(far(n))

    pair_term(0)
    value_step(0)

    @pl.loop(2, line)
    def _(n):
        tok_relayed(far(n))

    @pl.loop(2, line)
    def _(n):
        tok_landed(far(n))

    share(me)

    @pl.loop(1, line - 1)
    def _(tt):
        gather(tt - 1)
        pair_term(tt)

        @pl.when(tt < rounds)
        def _():
            conv_add(tt - 1)
            conv_copy(tt).start()

        value_step(tt)
        share_line(tt)

        @pl.when(tt == 1)
        def _():
            share_pair(0, False)

        @pl.when(tt > 1)
        def _():
            share_pair(tt - 1)

    gate_step(0)
    gather(line - 2)
    pair_term(line - 1)
    conv_add(rounds - 1)
    gate_step(1)
    share_line(line - 1)
    share_pair(line - 2)

    @pl.loop(2, line - 1)
    def _(tt):
        gate_step(tt)

    def arrive(slots, ru, rd, finish):
        low, high = slots.at[i], slots.at[line]

        @pl.when(has_down)
        def _():
            remote(low, low, xs, ru.at[i]).wait_recv()

        @pl.when(has_up)
        def _():
            remote(high, high, xs, rd.at[i]).wait_recv()

        @pl.when(has_down & has_up)
        def _():
            finish(low, high)

        @pl.when(jnp.logical_not(has_up))
        def _():
            finish(low)

        @pl.when(jnp.logical_not(has_down))
        def _():
            finish(high)

    term(False, other)
    arrive(sb.at[1 - j], bru.at[1 - j], brd.at[1 - j], lambda *refs: put(vx_out, *refs))
    cross = remote(vx_out, vx_in, xs, xr, other)
    cross.start()
    term(False, me)
    arrive(sb.at[j], bru.at[j], brd.at[j], lambda *refs: put(columns_of(vfin, split, wide_b), *refs))
    share_pair(line - 1)

    @pl.loop(0, n_fs)
    def _(o):
        @pl.loop(1, n_tp)
        def _(step):
            source = (tp + step) % n_tp
            remote(ig_send.at[source, o], ig_recv.at[source, o], ig_ss.at[source, o], ig_rs.at[source, o]).wait_recv()

    for o in range(n_fs):
        total = ig_send[tp, o].astype(F32)
        for step in range(1, n_tp):
            total = total + ig_recv[(tp + step) % n_tp, o].astype(F32)
        ig_sum[:, o * shard : (o + 1) * shard] = total.astype(BF16)
    conv_out[...] = csum[pl.ds(0, 3), :] * scale
    bias_out[...] = csum[pl.ds(3, 1), :] * scale

    term(True, me)
    put(acc, from_pair(i)())
    cross.wait_recv()

    def finish_value(cut):
        rest = pl.ds(split, wide_b)
        vfin[cut, rest] = (vfin[cut, rest] + vx_in[cut, :].astype(F32)) * scale

    each_rows(finish_value)

    def finish_gate(*refs):
        def body(cut):
            total = acc[cut, :]
            for ref in refs:
                total = total + ref[cut, :].astype(F32)
            total = total * scale
            gfin[cut, :] = total[:, split:]
            if split:
                vfin[cut, pl.ds(0, split)] = total[:, :split]

        each_rows(body)

    arrive(sa, aru, ard, finish_gate)

    part_b(me, bx, other).wait_send()
    cross.wait_send()

    @pl.loop(0, line)
    def _(d):
        @pl.loop(1, chips)
        def _(step):
            source = on_chip(step)
            tok_copy(d, tp, tok_ss.at[source, d], source).wait_send()
            tok_copy(d, source, tok_relay.at[source, d], twin).wait_send()

        tok_copy(d, tp, tok_relay.at[tp, d], twin).wait_send()
        pair_copy(d).wait_send()
        part_a(2 * d, ax, other).wait_send()

        @pl.when(has_up & (d <= i))
        def _():
            part_a(2 * d, a_up, up).wait_send()
            part_b(2 * d, b_up, up).wait_send()
            part_b(2 * d + 1, b_up, up).wait_send()

        @pl.when(has_down & (d >= i))
        def _():
            part_a(2 * d, a_down, down).wait_send()
            part_b(2 * d, b_down, down).wait_send()
            part_b(2 * d + 1, b_down, down).wait_send()

        @pl.when(d > i)
        def _():
            for jd in range(2):
                remote(sb.at[jd, d], sb.at[jd, d], bu.at[jd, d], bru.at[jd, d]).wait_send()
            remote(sa.at[d], sa.at[d], au.at[d], aru.at[d]).wait_send()

        @pl.when(d < i)
        def _():
            for jd in range(2):
                remote(sb.at[jd, d], sb.at[jd, d], bd.at[jd, d], brd.at[jd, d]).wait_send()
            remote(sa.at[d], sa.at[d], ad.at[d], ard.at[d]).wait_send()

    @pl.loop(0, n_fs)
    def _(o):
        @pl.loop(1, n_tp)
        def _(step):
            share_copy((tp + step) % n_tp, o).wait_send()


def on_device(
    tokens, gate_pre, value_pre, up_gate_w, up_value_w, conv_weight, conv_bias, hidden_grad
):
    n_fs, n_tp = lax.axis_size("fs"), lax.axis_size("tp")
    line = n_fs // 2
    rows, cols = gate_pre.shape
    own_tok, width = tokens.shape
    shard = up_gate_w.shape[0]
    rounds = n_fs.bit_length() - 1
    assert n_fs == 1 << rounds and line >= rounds + 1 and shard * n_fs == width
    scale = float(rows * n_fs) ** (-0.5)
    any_space = pl.BlockSpec(memory_space=pl.ANY)
    vmem = pl.BlockSpec(memory_space=pltpu.VMEM)
    dma = pltpu.SemaphoreType.DMA
    split = 0 if cols % LANES else cols * SPLIT // (11 * LANES) * LANES
    block, block_a, block_b = (shard, cols), (shard, cols + split), (shard, cols - split)
    input_grad, gate_out, value_out, conv, bias = pl.pallas_call(
        functools.partial(kernel, line, n_tp, split, scale),
        out_shape=(
            pltpu.VMEM((own_tok, width), BF16),
            pltpu.VMEM(block, F32),
            pltpu.VMEM(block, F32),
            pltpu.VMEM((3, cols), F32),
            pltpu.VMEM((1, cols), F32),
        ),
        in_specs=[any_space] * 6 + [vmem] * 2,
        out_specs=(vmem,) * 5,
        scratch_shapes=[
            pltpu.VMEM((n_fs, *block_a), BF16),
            pltpu.VMEM((n_fs, *block_b), BF16),
            pltpu.VMEM((own_tok, width), BF16),
            pltpu.VMEM((width, rows), BF16),
            pltpu.VMEM((PAD + rows, cols), BF16),
            pltpu.VMEM((rows, cols), BF16),
            pltpu.VMEM((max(rows, line * shard), cols + split), BF16),
            pltpu.VMEM((rows + 8, LANES), F32),
            pltpu.VMEM(block_a, F32),
            pltpu.VMEM((2, line + 1, *block_b), BF16),
            pltpu.VMEM((line + 1, *block_a), BF16),
            pltpu.VMEM((line, *block_a), BF16),
            pltpu.VMEM(block_b, BF16),
            pltpu.VMEM(block_b, BF16),
            pltpu.VMEM((n_tp, n_fs, own_tok, shard), BF16),
            pltpu.VMEM((n_tp, n_fs, own_tok, shard), BF16),
            pltpu.VMEM((rounds, 4, cols), F32),
            pltpu.VMEM((8, cols), F32),
            dma((7,)),
            *[dma((n_tp, line))] * 3,
            *[dma((line,))] * 3,
            dma((n_fs,)),
            dma((n_fs,)),
            dma((n_fs,)),
            dma((n_fs,)),
            dma((n_fs,)),
            *[dma((2, line))] * 4,
            *[dma((line,))] * 4,
            *[dma((line,))] * 2,
            dma,
            dma,
            *[dma((n_tp, n_fs))] * 2,
            *[dma((rounds,))] * 2,
        ],
        compiler_params=pltpu.CompilerParams(
            collective_id=0, has_side_effects=True, vmem_limit_bytes=60_000_000
        ),
        name="backward",
    )(
        tokens, gate_pre, value_pre, up_gate_w, up_value_w, hidden_grad,
        conv_weight, conv_bias.reshape(1, cols),
    )
    return (input_grad, gate_out, value_out, conv, bias.reshape(cols))


def solution(mesh):
    return jax.shard_map(
        on_device,
        mesh=mesh,
        in_specs=(
            P(("fs", "tp"), None),
            P("fs", "tp"),
            P("fs", "tp"),
            P("fs", "tp"),
            P("fs", "tp"),
            P(None, "tp"),
            P("tp"),
            P("fs", "tp"),
        ),
        out_specs=(P(("fs", "tp"), None), P("fs", "tp"), P("fs", "tp"), P(None, "tp"), P("tp")),
        check_vma=False,
    )
```

time: 225 us -> 194 us (0.86)
  the two profiles are of different devices: /device:TPU:17 before, /device:TPU:0 now
where the time goes in v2:
time: 194 us
  Pallas kernels  187 us (96%)
  local copies, waits for them, and re-layouts  5.07 us (3%)
    pallas_call x1, Pallas kernels, on_device(): pl.pallas_call(functools.partial(kernel, line, n_tp, split, scale), out_s...  187 us

profile of v2, /device:TPU:0, one launch (start us, length us, event | category | flops | bytes accessed | tf_op | source)
XLA Modules:
  0.0 193.8 jit_solution(2988055249307827484)
XLA Ops:
  0.6 1.3 reshape.16.bias
  1.9 187.4 %backward.1 = (bf16[256,2048]{1,0:T(8,128)(2,1)S(1)}, f32[256,1408]{1,0:T(8,128)S(1)}, f32[256,1408]{1,0:T(8,128)S(1)}, f32[3,1408]{1,0:T(4,128)S(1)}, f32[1,1408]{1,0:T(1,128)S(1)}) custom-call(bf16[256,2048]{1,0:T(8,128)(2,1)} %tok_hbm.1, bf16[1024,1408]{1,0:T(8,128)(2,1)} %gate_hbm.1, bf16[1024,1408]{1,0:T(8,128)(2,1)} %value_hbm.1, ...), custom_call_target="tpu_custom_call" | custom-call | tf_op jit(solution)/shard_map/backward/pallas_call | solution.py:611
  189.4 1.1 copy.18
  190.5 1.1 copy.19
  191.6 1.0 copy.17
  192.6 0.6 copy.20
  193.2 0.6 reduce

commit v3 on v2

v3 whole, which is shorter than its diff:
```python
import functools
import math
from types import SimpleNamespace

import jax
import jax.numpy as jnp
from jax import lax
from jax.experimental import pallas as pl
from jax.experimental.pallas import tpu as pltpu
from jax.sharding import PartitionSpec as P

MESH = pl.DeviceIdType.MESH
F32, BF16 = jnp.float32, jnp.bfloat16
PAD = 16
LANES = 128
SPLIT = 7
GROUPS = 3


def dot_rows(left, right):
    return lax.dot_general(left, right, (((1,), (0,)), ((), ())), preferred_element_type=F32)


def dot_cols(left, right):
    return lax.dot_general(left, right, (((1,), (1,)), ((), ())), preferred_element_type=F32)


def tiles(width, tile, body, first=0):
    whole = width // tile

    @pl.loop(0, whole)
    def _(n):
        body(pl.multiple_of(n * tile + first, LANES), tile)

    if width % tile:
        body(first + whole * tile, width % tile)


def groups_of(cols, split):
    width = split + cols
    if cols % LANES:
        edges = [0, width]
    else:
        edges = [width // LANES * g // GROUPS * LANES for g in range(GROUPS + 1)]
    pieces = []
    for first, last in zip(edges, edges[1:]):
        piece = []
        if first < split:
            piece.append((False, first, 0, min(last, split) - first))
        if last > split:
            at = max(first, split)
            piece.append((True, at - split, at - first, last - at))
        pieces.append((first, last - first, piece))
    return pieces


def kernel(
    line, n_tp, split, pieces, names, scale,
    tok_hbm, gate_hbm, value_hbm, wg_hbm, wv_hbm, hid_hbm, taps, bias,
    ig_sum, gfin, vfin, conv_out, bias_out, *scratch,
):
    own = SimpleNamespace(**dict(zip(names, scratch, strict=True)))
    wa, wb, tok, tok_t, pair_tok, gst, hst, vst = (
        own.wa, own.wb, own.tok, own.tok_t, own.pair_tok, own.gst, own.hst, own.vst
    )
    cgs, acc, csum, conv_recv, load_sem = own.cgs, own.acc, own.csum, own.conv_recv, own.load_sem
    tok_ss, tok_relay, tok_rs = own.tok_ss, own.tok_relay, own.tok_rs
    ig_send, ig_recv = own.ig_send, own.ig_recv
    me, tp = lax.axis_index("fs"), lax.axis_index("tp")
    i, j = me // 2, me % 2
    other = 2 * i + 1 - j
    up, down = me + 2, me - 2
    has_up, has_down = i < line - 1, i > 0
    n_fs = 2 * line
    rows, cols = hid_hbm.shape
    shard = wg_hbm.shape[0]
    own_tok, width = tok_hbm.shape
    rounds = n_fs.bit_length() - 1
    wide_b = cols - split

    def remote(src, dst, ss, rs, fs=None, to_tp=None):
        where = {"fs": me if fs is None else fs, "tp": tp if to_tp is None else to_tp}
        return pltpu.make_async_remote_copy(
            src_ref=src, dst_ref=dst, send_sem=ss, recv_sem=rs, device_id=where, device_id_type=MESH
        )

    def columns_of(ref, first, count):
        return ref if count == ref.shape[-1] else ref.at[:, pl.ds(first, count)]

    barrier = pltpu.get_barrier_semaphore()

    def greet(fs, to_tp):
        pl.semaphore_signal(barrier, inc=1, device_id={"fs": fs, "tp": to_tp}, device_id_type=MESH)

    greet(other, tp)

    @pl.when(has_up)
    def _():
        greet(up, tp)

    @pl.when(has_down)
    def _():
        greet(down, tp)

    for r in range(2, rounds):
        greet(me ^ (1 << r), tp)

    @pl.loop(1, n_tp)
    def _(step):
        greet(me, (tp + step) % n_tp)

    def part_a(o, ss, to):
        return remote(wa.at[o // 2], wa.at[o // 2], ss.at[o // 2], own.ra.at[o // 2], to)

    def part_b(o, ss, to):
        return remote(wb.at[o], wb.at[o], ss.at[o], own.rb.at[o], to)

    a_up, a_down, b_up, b_down, bx = own.a_up, own.a_down, own.b_up, own.b_down, own.bx

    def along(part, o, up_ss, down_ss, go_up, go_down):
        @pl.when(go_up)
        def _():
            part(o, up_ss, up).start()

        @pl.when(go_down)
        def _():
            part(o, down_ss, down).start()

    loads = [
        pltpu.make_async_copy(tok_hbm, tok, load_sem.at[0]),
        pltpu.make_async_copy(columns_of(wv_hbm, split, wide_b), wb.at[me], load_sem.at[1]),
        pltpu.make_async_copy(wg_hbm, columns_of(wa.at[i], split, cols), load_sem.at[2]),
        pltpu.make_async_copy(gate_hbm, gst.at[pl.ds(PAD, rows)], load_sem.at[3]),
        pltpu.make_async_copy(hid_hbm, hst, load_sem.at[4]),
        pltpu.make_async_copy(value_hbm, vst, load_sem.at[5]),
    ]
    if split:
        loads.insert(1, pltpu.make_async_copy(
            columns_of(wv_hbm, 0, split), columns_of(wa.at[i], 0, split), load_sem.at[6]
        ))
    for load in loads:
        load.start()

    met = 1 + (rounds - 2) + (n_tp - 1) + jnp.where(has_up, 1, 0) + jnp.where(has_down, 1, 0)
    pl.semaphore_wait(barrier, met)

    weights = 4 if split else 3
    for load in loads[1:weights]:
        load.wait()
    part_b(me, bx, other).start()
    along(part_a, me, a_up, a_down, has_up, has_down)
    along(part_b, me, b_up, b_down, has_up, has_down)

    loads[0].wait()
    turn = 256

    @pl.loop(0, width // turn)
    def _(n):
        at = pl.multiple_of(n * turn, turn)
        tok_t[pl.ds(at, turn), pl.ds(pl.multiple_of(tp * own_tok, own_tok), own_tok)] = tok[
            :, pl.ds(at, turn)
        ].T

    def tok_piece(d, source):
        return tok_t.at[
            pl.ds(pl.multiple_of(d * 2 * shard, 2 * shard), 2 * shard),
            pl.ds(pl.multiple_of(source * own_tok, own_tok), own_tok),
        ]

    def far(n):
        mirror = 2 * i >= line
        at = jnp.where(mirror, line - 1 - i, i)
        d = line - 1 - n
        d = jnp.where(d > at, d, jnp.where(d == 0, at, d - 1))
        return jnp.where(mirror, line - 1 - d, d)

    def tok_copy(d, source, ss, to):
        return remote(tok_piece(d, source), tok_piece(d, source), ss, tok_rs.at[source, d], to_tp=to)

    core, twin, chips = tp % 2, tp + 1 - 2 * (tp % 2), n_tp // 2

    def on_chip(step):
        return 2 * ((tp // 2 + step) % chips) + core

    @pl.loop(0, line)
    def _(n):
        d = far(n)

        @pl.loop(1, chips)
        def _(step):
            tok_copy(d, tp, tok_ss.at[on_chip(step), d], on_chip(step)).start()

        tok_copy(d, tp, tok_relay.at[tp, d], twin).start()

    def tok_relayed(d):
        @pl.loop(1, chips)
        def _(step):
            source = on_chip(step)
            tok_copy(d, source, tok_relay.at[source, d], twin).wait_recv()
            tok_copy(d, source, tok_relay.at[source, d], twin).start()

    def tok_landed(d):
        @pl.loop(0, chips)
        def _(step):
            source = on_chip(step) + twin - tp
            tok_copy(d, source, tok_relay.at[source, d], twin).wait_recv()

    def pair_piece(d):
        return remote(
            tok_t.at[
                pl.ds(pl.multiple_of((2 * d + 1 - j) * shard, shard), shard),
                pl.ds(pl.multiple_of(tp * own_tok, own_tok), own_tok),
            ],
            pair_tok.at[
                pl.ds(pl.multiple_of(d * shard, shard), shard),
                pl.ds(pl.multiple_of(tp * own_tok, own_tok), own_tok),
            ],
            own.px_ss.at[d], own.px_rs.at[d], other,
        )

    def pair_cols(source, ss, to):
        part = pair_tok.at[:, pl.ds(pl.multiple_of(source * own_tok, own_tok), own_tok)]
        return remote(part, part, ss, own.pt_rs.at[source], to_tp=to)

    def pair_tokens_out():
        @pl.loop(0, line)
        def _(d):
            pair_piece(d).wait_recv()

        @pl.loop(1, chips)
        def _(step):
            pair_cols(tp, own.pt_ss.at[on_chip(step)], on_chip(step)).start()

        pair_cols(tp, own.pt_relay.at[tp], twin).start()

    def pair_tokens_in():
        @pl.loop(1, chips)
        def _(step):
            source = on_chip(step)
            pair_cols(source, own.pt_relay.at[source], twin).wait_recv()
            pair_cols(source, own.pt_relay.at[source], twin).start()

        @pl.loop(0, chips)
        def _(step):
            source = on_chip(step) + twin - tp
            pair_cols(source, own.pt_relay.at[source], twin).wait_recv()

    @pl.loop(0, line)
    def _(d):
        pair_piece(d).start()

    for load in loads[weights:]:
        load.wait()
    chunk = 64
    root = math.sqrt(2.0 / math.pi)

    def elementwise(at, size):
        cut = pl.ds(at, size)
        gst[pl.ds(0, PAD), cut] = jnp.zeros((PAD, size), BF16)
        w0, w1, w2 = (taps[pl.ds(k, 1), cut] for k in range(3))
        b = bias[cut].reshape(1, size)

        def forward(n, sums):
            r = pl.multiple_of(n * chunk, chunk)
            wide = gst[pl.ds(r, PAD + chunk), cut].astype(F32)
            x0 = wide[PAD:]
            x1 = pltpu.roll(wide, 1, 0)[PAD:]
            x2 = pltpu.roll(wide, 2, 0)[PAD:]
            z = b + w0 * x2 + w1 * x1 + w2 * x0
            sq = z * z
            th = jnp.tanh(root * (z + 0.044715 * (sq * z)))
            cdf = 0.5 * (1.0 + th)
            h = hst[pl.ds(r, chunk), cut].astype(F32)
            v = vst[pl.ds(r, chunk), cut].astype(F32)
            hst[pl.ds(r, chunk), cut] = (h * (z * cdf)).astype(BF16)
            slope = cdf + (0.5 * z) * (1.0 - th * th) * (root + (3.0 * 0.044715 * root) * sq)
            cg = slope * (h * v)
            cgs[pl.ds(r, chunk), pl.ds(0, size)] = cg

            def fold(term):
                return jnp.sum(term.reshape(chunk // 8, 8, size), axis=0)

            return tuple(s + fold(t) for s, t in zip(sums, (cg * x2, cg * x1, cg * x0, cg)))

        zero = jnp.zeros((8, size), F32)
        sums = lax.fori_loop(0, rows // chunk, forward, (zero,) * 4)
        for k in range(4):
            csum[pl.ds(k, 1), cut] = jnp.sum(sums[k], axis=0, keepdims=True)
        cgs[pl.ds(rows, 8), pl.ds(0, size)] = jnp.zeros((8, size), F32)

        @pl.loop(0, rows // chunk)
        def _(n):
            r = pl.multiple_of(n * chunk, chunk)
            wide = cgs[pl.ds(r, chunk + 8), pl.ds(0, size)]
            g1 = pltpu.roll(wide, chunk + 7, 0)[:chunk]
            g2 = pltpu.roll(wide, chunk + 6, 0)[:chunk]
            gst[pl.ds(PAD + r, chunk), cut] = (w2 * wide[:chunk] + w1 * g1 + w0 * g2).astype(BF16)

    def grad_ref(is_gate, at, size):
        ref = gst.at[pl.ds(PAD, rows)] if is_gate else hst
        return columns_of(ref, at, size)

    def grad_copies(g):
        _, _, segments = pieces[g]
        into = getattr(own, f"pg{g}")
        return [
            remote(
                grad_ref(is_gate, at, size), columns_of(into, to, size),
                own.g_ss.at[g, n], own.g_rs.at[g, n], other,
            )
            for n, (is_gate, at, to, size) in enumerate(segments)
        ]

    ready = 0
    for g, (_, _, segments) in enumerate(pieces):
        need = max(at + size for _, at, _, size in segments)
        if need > ready:
            tiles(need - ready, LANES, elementwise, ready)
            ready = need
        for copy in grad_copies(g):
            copy.start()
    if ready < cols:
        tiles(cols - ready, LANES, elementwise, ready)

    def conv_copy(r):
        return remote(csum.at[pl.ds(0, 4)], conv_recv.at[r], own.cs.at[r], own.cr.at[r], me ^ (1 << r))

    def conv_add(r):
        conv_copy(r).wait_send()
        conv_copy(r).wait_recv()
        csum[pl.ds(0, 4), :] += conv_recv[r]

    turns = [*range(1, rounds), 0]
    conv_copy(turns[0]).start()

    part_b(other, bx, other).wait_recv()
    along(part_b, other, b_up, b_down, has_up, has_down)

    def gather(t):
        low, high = i - t - 1, i + t + 1

        @pl.when(low >= 0)
        def _():
            o = 2 * low + j
            part_a(o, a_up, up).wait_recv()
            along(part_a, o, a_up, a_down, has_up, False)

        @pl.when(high < line)
        def _():
            o = 2 * high + j
            part_a(o, a_down, down).wait_recv()
            along(part_a, o, a_up, a_down, False, has_down)

        for flip in range(2):
            jd = j if flip == 0 else 1 - j

            @pl.when(low >= 0)
            def _():
                o = 2 * low + jd
                part_b(o, b_up, up).wait_recv()
                along(part_b, o, b_up, b_down, has_up, False)

            @pl.when(high < line)
            def _():
                o = 2 * high + jd
                part_b(o, b_down, down).wait_recv()
                along(part_b, o, b_up, b_down, False, has_down)

    def left_rows(o):
        return pl.ds(pl.multiple_of(o * shard, shard), shard)

    def term_b(o):
        def one(at, size):
            grad = hst[:, pl.ds(pl.multiple_of(at + split, LANES), size)]
            acc[:, pl.ds(at, size)] = dot_rows(tok_t[left_rows(o), :], grad)

        tiles(wide_b, 256, one)

    def term_a(g, d):
        from_pair = getattr(own, f"pg{g}")
        for is_gate, first, to, count in pieces[g][2]:
            def one(at, size):
                cut = pl.ds(at, size)
                if is_gate:
                    grad = gst[pl.ds(PAD, rows), pl.ds(pl.multiple_of(at - to + first, LANES), size)]
                else:
                    grad = hst[:, pl.ds(pl.multiple_of(at - to + first, LANES), size)]
                total = dot_rows(tok_t[left_rows(2 * d + j), :], grad)
                acc[:, cut] = total + dot_rows(pair_tok[left_rows(d), :], from_pair[:, cut])

            tiles(count, 256, one, to)

    step_rows = 16

    def each_rows(body):
        @pl.loop(0, shard // step_rows)
        def _(n):
            body(pl.ds(pl.multiple_of(n * step_rows, step_rows), step_rows))

    def put(dst, *more):
        span = pl.ds(0, dst.shape[-1])

        def body(cut):
            total = acc[cut, span]
            for ref in more:
                total = total + ref[cut, :].astype(F32)
            dst[cut, span] = total.astype(dst.dtype)

        each_rows(body)

    def unit(w, jd=0):
        if w == 0:
            return own.sb.at[jd], own.sb_ss.at[jd], own.sb_rs.at[jd], lambda d: term_b(2 * d + jd)
        return getattr(own, f"sa{w - 1}"), own.sa_ss.at[w - 1], own.sa_rs.at[w - 1], lambda d: term_a(w - 1, d)

    def level(w, h, jd=0):
        slots, ss, rs, term = unit(w, jd)
        going_up, going_down = i == h, i == line - 1 - h

        @pl.when(going_up | going_down)
        def _():
            @pl.loop(0, line - 1 - h)
            def _(n):
                d = jnp.where(going_up, line - 1 - n, n)
                ahead = jnp.where(going_up, i + 1, i - 1)
                to = jnp.where(going_down & (d == ahead), line, d)
                slot = slots.at[d]
                term(d)
                if h:
                    remote(slot, slot, ss.at[d], rs.at[d]).wait_recv()
                    put(slot, slot)
                else:
                    put(slot)
                remote(slot, slots.at[to], ss.at[d], rs.at[to], 2 * ahead + j).start()

    def arrive(w, jd, finish):
        slots, ss, rs, term = unit(w, jd)
        low, high = slots.at[i], slots.at[line]
        term(i)

        @pl.when(has_down)
        def _():
            remote(low, low, ss.at[i], rs.at[i]).wait_recv()

        @pl.when(has_up)
        def _():
            remote(high, high, ss.at[i], rs.at[line]).wait_recv()

        @pl.when(has_down & has_up)
        def _():
            finish(low, high)

        @pl.when(jnp.logical_not(has_up))
        def _():
            finish(low)

        @pl.when(jnp.logical_not(has_down))
        def _():
            finish(high)

    def share_copy(k, o):
        return remote(ig_send.at[k, o], ig_recv.at[tp, o], own.ig_ss.at[k, o], own.ig_rs.at[tp, o], to_tp=k)

    def share(at, column):
        o = 2 * at + column

        @pl.loop(1, n_tp + 1)
        def _(step):
            k = (tp + step) % n_tp
            start = pl.multiple_of(k * own_tok, own_tok)
            here = pl.ds(start, own_tok)
            part = dot_cols(hst[here, pl.ds(split, wide_b)], wb[o])
            if column is j:
                part = part + dot_cols(gst[pl.ds(PAD + start, own_tok), :], wa[at, :, pl.ds(split, cols)])
                if split:
                    part = part + dot_cols(hst[here, pl.ds(0, split)], wa[at, :, pl.ds(0, split)])
            ig_send[k, o] = part.astype(BF16)

            @pl.when(k != tp)
            def _():
                share_copy(k, o).start()

    def share_far(t):
        for at in (i - t, i + t):
            @pl.when((at >= 0) & (at < line))
            def _():
                share(at, j)
                share(at, 1 - j)

    def pair_share_copy(k):
        return remote(own.pi_send.at[k], own.pi_recv.at[tp], own.pi_ss.at[k], own.pi_rs.at[tp], to_tp=k)

    def pair_shares():
        @pl.loop(1, n_tp + 1)
        def _(step):
            k = (tp + step) % n_tp
            here = pl.ds(pl.multiple_of(k * own_tok, own_tok), own_tok)

            @pl.loop(0, line)
            def _(at):
                part = None
                for g, (first, size, _) in enumerate(pieces):
                    one = dot_cols(getattr(own, f"pg{g}")[here, :], wa[at, :, pl.ds(first, size)])
                    part = one if part is None else part + one
                own.pi_send[k, at] = part.astype(BF16)

            @pl.when(k != tp)
            def _():
                pair_share_copy(k).start()

    back = remote(own.ret_out, own.ret_in, own.ret_ss, own.ret_rs, other)

    def pair_shares_back():
        @pl.loop(1, n_tp)
        def _(step):
            source = (tp + step) % n_tp
            remote(own.pi_send.at[source], own.pi_recv.at[source], own.pi_ss.at[source], own.pi_rs.at[source]).wait_recv()

        @pl.loop(0, line)
        def _(at):
            total = own.pi_send[tp, at].astype(F32)
            for step in range(1, n_tp):
                total = total + own.pi_recv[(tp + step) % n_tp, at].astype(F32)
            own.ret_out[at] = total.astype(BF16)

        back.start()

    def finish_piece(g):
        def finish(*refs):
            def body(cut):
                total = acc[cut, pl.ds(0, pieces[g][1])]
                for ref in refs:
                    total = total + ref[cut, :].astype(F32)
                total = total * scale
                for is_gate, at, to, size in pieces[g][2]:
                    (gfin if is_gate else vfin)[cut, pl.ds(at, size)] = total[:, to : to + size]

            each_rows(body)

        arrive(g + 1, 0, finish)

    @pl.loop(0, line)
    def _(n):
        tok_relayed(far(n))

    pair_tokens_out()

    @pl.loop(0, line)
    def _(n):
        tok_landed(far(n))

    waves = len(pieces) + 1
    cross = remote(own.vx_out, own.vx_in, own.xs, own.xr, other)
    for s in range(waves + line - 2):
        for w in range(waves):
            if w and s == w:
                if w == 1:
                    pair_tokens_in()
                for copy in grad_copies(w - 1):
                    copy.wait_recv()
            if 0 <= s - w < line - 1:
                for jd in range(2 if w == 0 else 1):
                    level(w, s - w, jd)
        if s == 0:
            share(i, j)
            share(i, 1 - j)
        if s < line - 1:
            gather(s)
            share_far(s + 1)
        if s % 2 == 0 and s // 2 < rounds:
            conv_add(turns[s // 2])
            if s // 2 + 1 < rounds:
                conv_copy(turns[s // 2 + 1]).start()
        if s == max(waves - 1, line - 2):
            pair_shares()
        if s == line - 1:
            for mine in (False, True):
                column = j if mine else 1 - j
                finish = (
                    (lambda *refs: put(columns_of(vfin, split, wide_b), *refs))
                    if mine
                    else (lambda *refs: put(own.vx_out, *refs))
                )
                arrive(0, column, finish)
                if not mine:
                    cross.start()
        g = s - line
        if 0 <= g < len(pieces) - 1:
            finish_piece(g)

    conv_out[...] = csum[pl.ds(0, 3), :] * scale
    bias_out[...] = (csum[pl.ds(3, 1), :] * scale).reshape(cols)
    pair_shares_back()
    for g in range(max(0, waves - 2), len(pieces)):
        finish_piece(g)
    cross.wait_recv()

    def finish_value(cut):
        rest = pl.ds(split, wide_b)
        vfin[cut, rest] = (vfin[cut, rest] + own.vx_in[cut, :].astype(F32)) * scale

    each_rows(finish_value)

    @pl.loop(0, n_fs)
    def _(o):
        @pl.loop(1, n_tp)
        def _(step):
            source = (tp + step) % n_tp
            remote(
                ig_send.at[source, o], ig_recv.at[source, o], own.ig_ss.at[source, o], own.ig_rs.at[source, o]
            ).wait_recv()

    back.wait_recv()
    for o in range(n_fs):
        total = ig_send[tp, o].astype(F32)
        for step in range(1, n_tp):
            total = total + ig_recv[(tp + step) % n_tp, o].astype(F32)
        total = total + jnp.where(o % 2 != j, own.ret_in[o // 2].astype(F32), 0.0)
        ig_sum[:, o * shard : (o + 1) * shard] = total.astype(BF16)

    part_b(me, bx, other).wait_send()
    cross.wait_send()
    back.wait_send()
    for g in range(len(pieces)):
        for copy in grad_copies(g):
            copy.wait_send()
    pair_cols(tp, own.pt_relay.at[tp], twin).wait_send()

    @pl.loop(1, chips)
    def _(step):
        source = on_chip(step)
        pair_cols(tp, own.pt_ss.at[source], source).wait_send()
        pair_cols(source, own.pt_relay.at[source], twin).wait_send()

    @pl.loop(1, n_tp)
    def _(step):
        pair_share_copy((tp + step) % n_tp).wait_send()

    @pl.loop(0, line)
    def _(d):
        @pl.loop(1, chips)
        def _(step):
            source = on_chip(step)
            tok_copy(d, tp, tok_ss.at[source, d], source).wait_send()
            tok_copy(d, source, tok_relay.at[source, d], twin).wait_send()

        tok_copy(d, tp, tok_relay.at[tp, d], twin).wait_send()
        pair_piece(d).wait_send()

        @pl.when(has_up & (d <= i))
        def _():
            part_a(2 * d, a_up, up).wait_send()
            part_b(2 * d, b_up, up).wait_send()
            part_b(2 * d + 1, b_up, up).wait_send()

        @pl.when(has_down & (d >= i))
        def _():
            part_a(2 * d, a_down, down).wait_send()
            part_b(2 * d, b_down, down).wait_send()
            part_b(2 * d + 1, b_down, down).wait_send()

        @pl.when(d != i)
        def _():
            for w in range(waves):
                for jd in range(2 if w == 0 else 1):
                    slots, ss, rs, _ = unit(w, jd)
                    remote(slots.at[d], slots.at[d], ss.at[d], rs.at[d]).wait_send()

    @pl.loop(0, n_fs)
    def _(o):
        @pl.loop(1, n_tp)
        def _(step):
            share_copy((tp + step) % n_tp, o).wait_send()


def scratch_of(line, n_tp, split, pieces, rows, cols, own_tok, width, shard, rounds):
    n_fs, parts, wide_b = 2 * line, len(pieces), cols - split
    dma = pltpu.SemaphoreType.DMA
    widest = max([wide_b] + [size for _, size, _ in pieces])
    table = dict(
        wa=pltpu.VMEM((line, shard, cols + split), BF16),
        wb=pltpu.VMEM((n_fs, shard, wide_b), BF16),
        tok=pltpu.VMEM((own_tok, width), BF16),
        tok_t=pltpu.VMEM((width, rows), BF16),
        pair_tok=pltpu.VMEM((line * shard, rows), BF16),
        gst=pltpu.VMEM((PAD + rows, cols), BF16),
        hst=pltpu.VMEM((rows, cols), BF16),
        vst=pltpu.VMEM((rows, cols), BF16),
        cgs=pltpu.VMEM((rows + 8, LANES), F32),
        acc=pltpu.VMEM((shard, widest), F32),
        sb=pltpu.VMEM((2, line + 1, shard, wide_b), BF16),
        vx_out=pltpu.VMEM((shard, wide_b), BF16),
        vx_in=pltpu.VMEM((shard, wide_b), BF16),
        ig_send=pltpu.VMEM((n_tp, n_fs, own_tok, shard), BF16),
        ig_recv=pltpu.VMEM((n_tp, n_fs, own_tok, shard), BF16),
        pi_send=pltpu.VMEM((n_tp, line, own_tok, shard), BF16),
        pi_recv=pltpu.VMEM((n_tp, line, own_tok, shard), BF16),
        ret_out=pltpu.VMEM((line, own_tok, shard), BF16),
        ret_in=pltpu.VMEM((line, own_tok, shard), BF16),
        conv_recv=pltpu.VMEM((rounds, 4, cols), F32),
        csum=pltpu.VMEM((8, cols), F32),
        load_sem=dma((7,)),
        tok_ss=dma((n_tp, line)), tok_relay=dma((n_tp, line)), tok_rs=dma((n_tp, line)),
        px_ss=dma((line,)), px_rs=dma((line,)),
        pt_ss=dma((n_tp,)), pt_relay=dma((n_tp,)), pt_rs=dma((n_tp,)),
        a_up=dma((line,)), a_down=dma((line,)), ra=dma((line,)),
        b_up=dma((n_fs,)), b_down=dma((n_fs,)), bx=dma((n_fs,)), rb=dma((n_fs,)),
        g_ss=dma((parts, 2)), g_rs=dma((parts, 2)),
        sb_ss=dma((2, line)), sb_rs=dma((2, line + 1)),
        sa_ss=dma((parts, line)), sa_rs=dma((parts, line + 1)),
        xs=dma, xr=dma, ret_ss=dma, ret_rs=dma,
        ig_ss=dma((n_tp, n_fs)), ig_rs=dma((n_tp, n_fs)),
        pi_ss=dma((n_tp,)), pi_rs=dma((n_tp,)),
        cs=dma((rounds,)), cr=dma((rounds,)),
    )
    for g, (_, size, _) in enumerate(pieces):
        table[f"pg{g}"] = pltpu.VMEM((rows, size), BF16)
        table[f"sa{g}"] = pltpu.VMEM((line + 1, shard, size), BF16)
    return table


def on_device(
    tokens, gate_pre, value_pre, up_gate_w, up_value_w, conv_weight, conv_bias, hidden_grad
):
    n_fs, n_tp = lax.axis_size("fs"), lax.axis_size("tp")
    line = n_fs // 2
    rows, cols = gate_pre.shape
    own_tok, width = tokens.shape
    shard = up_gate_w.shape[0]
    rounds = n_fs.bit_length() - 1
    assert n_fs == 1 << rounds and line >= max(4, rounds) and shard * n_fs == width and n_tp % 2 == 0
    scale = float(rows * n_fs) ** (-0.5)
    split = 0 if cols % LANES else cols * SPLIT // (11 * LANES) * LANES
    pieces = groups_of(cols, split)
    table = scratch_of(line, n_tp, split, pieces, rows, cols, own_tok, width, shard, rounds)
    any_space = pl.BlockSpec(memory_space=pl.ANY)
    vmem = pl.BlockSpec(memory_space=pltpu.VMEM)
    input_grad, gate_out, value_out, conv, bias = pl.pallas_call(
        functools.partial(kernel, line, n_tp, split, pieces, tuple(table), scale),
        out_shape=(
            pltpu.VMEM((own_tok, width), BF16),
            pltpu.VMEM((shard, cols), F32),
            pltpu.VMEM((shard, cols), F32),
            pltpu.VMEM((3, cols), F32),
            pltpu.VMEM((cols,), F32),
        ),
        in_specs=[any_space] * 6 + [vmem] * 2,
        out_specs=(vmem,) * 5,
        scratch_shapes=list(table.values()),
        compiler_params=pltpu.CompilerParams(
            collective_id=0, has_side_effects=True, vmem_limit_bytes=61_000_000
        ),
        name="backward",
    )(
        tokens, gate_pre, value_pre, up_gate_w, up_value_w, hidden_grad,
        conv_weight, conv_bias,
    )
    return (input_grad, gate_out, value_out, conv, bias)


def solution(mesh):
    return jax.shard_map(
        on_device,
        mesh=mesh,
        in_specs=(
            P(("fs", "tp"), None),
            P("fs", "tp"),
            P("fs", "tp"),
            P("fs", "tp"),
            P("fs", "tp"),
            P(None, "tp"),
            P("tp"),
            P("fs", "tp"),
        ),
        out_specs=(P(("fs", "tp"), None), P("fs", "tp"), P("fs", "tp"), P(None, "tp"), P("tp")),
        check_vma=False,
    )
```

time: 194 us -> 171 us (0.88)
  the two profiles are of different devices: /device:TPU:0 before, /device:TPU:16 now
where the time goes in v3:
time: 171 us
  Pallas kernels  166 us (97%)
  local copies, waits for them, and re-layouts  4.38 us (3%)
    pallas_call x1, Pallas kernels, on_device(): pl.pallas_call(functools.partial(kernel, line, n_tp, split, pieces, tuple...  166 us
    unnamed x5, local copies, waits for them, and re-layouts  4.38 us

profile of v3, /device:TPU:16, one launch (start us, length us, event | category | flops | bytes accessed | tf_op | source)
XLA Modules:
  0.0 170.9 jit_solution(2059446984033398760)
XLA Ops:
  0.6 165.9 %backward.1 = (bf16[256,2048]{1,0:T(8,128)(2,1)S(1)}, f32[256,1408]{1,0:T(8,128)S(1)}, f32[256,1408]{1,0:T(8,128)S(1)}, f32[3,1408]{1,0:T(4,128)S(1)}, f32[1408]{0:T(1024)S(1)}) custom-call(bf16[256,2048]{1,0:T(8,128)(2,1)} %tok_hbm.1, bf16[1024,1408]{1,0:T(8,128)(2,1)} %gate_hbm.1, bf16[1024,1408]{1,0:T(8,128)(2,1)} %value_hbm.1, bf16[256,1408]{1,0:T(8,128)(2,1)} %wg_hbm.1, ...), custom_call_target="tpu_custom_call" | custom-call | tf_op jit(solution)/shard_map/backward/pallas_call | solution.py:738
  166.6 1.0 copy.18
  167.5 0.6 copy.22
  168.1 0.6 copy.21
  168.8 1.1 copy.19
  169.8 1.1 copy.20

commit v4 on v3

--- a/solution.py
+++ b/solution.py
@@ -487,43 +487,46 @@
                 share(at, j)
                 share(at, 1 - j)
 
-    def pair_share_copy(k):
-        return remote(own.pi_send.at[k], own.pi_recv.at[tp], own.pi_ss.at[k], own.pi_rs.at[tp], to_tp=k)
+    def pair_share_copy(k, at):
+        return remote(own.pi_send.at[k, at], own.pi_recv.at[tp, at], own.pi_ss.at[k, at], own.pi_rs.at[tp, at], to_tp=k)
 
     def pair_shares():
-        @pl.loop(1, n_tp + 1)
-        def _(step):
-            k = (tp + step) % n_tp
-            here = pl.ds(pl.multiple_of(k * own_tok, own_tok), own_tok)
-
-            @pl.loop(0, line)
-            def _(at):
+        @pl.loop(0, line)
+        def _(at):
+            @pl.loop(0, n_tp)
+            def _(n):
+                k = 2 * ((tp // 2 + 1 + n // 2) % chips) + (core + n + 1) % 2
+                here = pl.ds(pl.multiple_of(k * own_tok, own_tok), own_tok)
                 part = None
                 for g, (first, size, _) in enumerate(pieces):
                     one = dot_cols(getattr(own, f"pg{g}")[here, :], wa[at, :, pl.ds(first, size)])
                     part = one if part is None else part + one
                 own.pi_send[k, at] = part.astype(BF16)
 
-            @pl.when(k != tp)
-            def _():
-                pair_share_copy(k).start()
-
-    back = remote(own.ret_out, own.ret_in, own.ret_ss, own.ret_rs, other)
-
-    def pair_shares_back():
-        @pl.loop(1, n_tp)
-        def _(step):
-            source = (tp + step) % n_tp
-            remote(own.pi_send.at[source], own.pi_recv.at[source], own.pi_ss.at[source], own.pi_rs.at[source]).wait_recv()
-
-        @pl.loop(0, line)
+                @pl.when(k != tp)
+                def _():
+                    pair_share_copy(k, at).start()
+
+    def back(at):
+        return remote(own.ret_out.at[at], own.ret_in.at[at], own.ret_ss.at[at], own.ret_rs.at[at], other)
+
+    def pair_shares_back(first, last):
+        @pl.loop(first, last)
         def _(at):
+            @pl.loop(1, n_tp)
+            def _(step):
+                pair_share_copy((tp + step) % n_tp, at).wait_send()
+                source = (tp + step) % n_tp
+                remote(
+                    own.pi_send.at[source, at], own.pi_recv.at[source, at],
+                    own.pi_ss.at[source, at], own.pi_rs.at[source, at],
+                ).wait_recv()
+
             total = own.pi_send[tp, at].astype(F32)
             for step in range(1, n_tp):
                 total = total + own.pi_recv[(tp + step) % n_tp, at].astype(F32)
             own.ret_out[at] = total.astype(BF16)
-
-        back.start()
+            back(at).start()
 
     def finish_piece(g):
         def finish(*refs):
@@ -551,8 +554,12 @@
 
     waves = len(pieces) + 1
     cross = remote(own.vx_out, own.vx_in, own.xs, own.xr, other)
+    returned = 0
     for s in range(waves + line - 2):
         for w in range(waves):
+            if s == line and w == waves - 1 and s > max(waves - 1, line - 2):
+                pair_shares_back(returned, returned + 1)
+                returned += 1
             if w and s == w:
                 if w == 1:
                     pair_tokens_in()
@@ -584,14 +591,17 @@
                 arrive(0, column, finish)
                 if not mine:
                     cross.start()
+        if s >= line - 1 and s >= waves - 1 and returned < line:
+            pair_shares_back(returned, returned + 1)
+            returned += 1
         g = s - line
         if 0 <= g < len(pieces) - 1:
             finish_piece(g)
 
     conv_out[...] = csum[pl.ds(0, 3), :] * scale
     bias_out[...] = (csum[pl.ds(3, 1), :] * scale).reshape(cols)
-    pair_shares_back()
-    for g in range(max(0, waves - 2), len(pieces)):
+    pair_shares_back(returned, line)
+    for g in range(max(0, waves - 2), len(pieces) - 1):
         finish_piece(g)
     cross.wait_recv()
 
@@ -610,17 +620,19 @@
                 ig_send.at[source, o], ig_recv.at[source, o], own.ig_ss.at[source, o], own.ig_rs.at[source, o]
             ).wait_recv()
 
-    back.wait_recv()
     for o in range(n_fs):
+        if o % 2 == 0:
+            back(o // 2).wait_recv()
         total = ig_send[tp, o].astype(F32)
         for step in range(1, n_tp):
             total = total + ig_recv[(tp + step) % n_tp, o].astype(F32)
         total = total + jnp.where(o % 2 != j, own.ret_in[o // 2].astype(F32), 0.0)
         ig_sum[:, o * shard : (o + 1) * shard] = total.astype(BF16)
 
+    finish_piece(len(pieces) - 1)
+
     part_b(me, bx, other).wait_send()
     cross.wait_send()
-    back.wait_send()
     for g in range(len(pieces)):
         for copy in grad_copies(g):
             copy.wait_send()
@@ -632,10 +644,6 @@
         pair_cols(tp, own.pt_ss.at[source], source).wait_send()
         pair_cols(source, own.pt_relay.at[source], twin).wait_send()
 
-    @pl.loop(1, n_tp)
-    def _(step):
-        pair_share_copy((tp + step) % n_tp).wait_send()
-
     @pl.loop(0, line)
     def _(d):
         @pl.loop(1, chips)
@@ -646,6 +654,7 @@
 
         tok_copy(d, tp, tok_relay.at[tp, d], twin).wait_send()
         pair_piece(d).wait_send()
+        back(d).wait_send()
 
         @pl.when(has_up & (d <= i))
         def _():
@@ -708,9 +717,9 @@
         g_ss=dma((parts, 2)), g_rs=dma((parts, 2)),
         sb_ss=dma((2, line)), sb_rs=dma((2, line + 1)),
         sa_ss=dma((parts, line)), sa_rs=dma((parts, line + 1)),
-        xs=dma, xr=dma, ret_ss=dma, ret_rs=dma,
+        xs=dma, xr=dma, ret_ss=dma((line,)), ret_rs=dma((line,)),
         ig_ss=dma((n_tp, n_fs)), ig_rs=dma((n_tp, n_fs)),
-        pi_ss=dma((n_tp,)), pi_rs=dma((n_tp,)),
+        pi_ss=dma((n_tp, line)), pi_rs=dma((n_tp, line)),
         cs=dma((rounds,)), cr=dma((rounds,)),
     )
     for g, (_, size, _) in enumerate(pieces):

time: 171 us -> 168 us (0.982)
  the two profiles are of different devices: /device:TPU:16 before, /device:TPU:0 now
where the time goes in v4:
time: 168 us; the launch traced here: 167 us
  Pallas kernels  162 us (96%)
  local copies, waits for them, and re-layouts  4.38 us (3%)
    pallas_call x1, Pallas kernels, on_device(): pl.pallas_call(functools.partial(kernel, line, n_tp, split, pieces, tuple...  162 us
    unnamed x5, local copies, waits for them, and re-layouts  4.38 us

profile of v4, /device:TPU:0, one launch (start us, length us, event | category | flops | bytes accessed | tf_op | source)
XLA Modules:
  0.0 167.4 jit_solution(11412621978472435359)
XLA Ops:
  0.6 162.4 %backward.1 = (bf16[256,2048]{1,0:T(8,128)(2,1)S(1)}, f32[256,1408]{1,0:T(8,128)S(1)}, f32[256,1408]{1,0:T(8,128)S(1)}, f32[3,1408]{1,0:T(4,128)S(1)}, f32[1408]{0:T(1024)S(1)}) custom-call(bf16[256,2048]{1,0:T(8,128)(2,1)} %tok_hbm.1, bf16[1024,1408]{1,0:T(8,128)(2,1)} %gate_hbm.1, bf16[1024,1408]{1,0:T(8,128)(2,1)} %value_hbm.1, bf16[256,1408]{1,0:T(8,128)(2,1)} %wg_hbm.1, ...), custom_call_target="tpu_custom_call" | custom-call | tf_op jit(solution)/shard_map/backward/pallas_call | solution.py:747
  163.0 1.0 copy.18
  164.0 0.6 copy.22
  164.6 0.6 copy.21
  165.2 1.1 copy.19
  166.3 1.1 copy.20
